TPU v7x, 256 devices: a whole 4x4x8 slice. The times are simulated.
256 devices in a mesh: ep: 32 (over z, x), tp: 8 (over y, core).
Axes of the slice: x: 4, y: 4, z: 8, core: 2. Of those that a mesh axis runs over, the one named last changes fastest.
Arguments:
- tokens: bfloat16 [3072, 4096], P('ep'), may hold values from -6 to 6
- mix_gain: float32 [4096], replicated, may hold values from 0.1 to 1.9
- ffn_gain: float32 [4096], replicated, may hold values from 0.1 to 1.9
- in_proj: bfloat16 [4096, 1024], P(None, 'tp'), may hold values from -0.09375 to 0.09375
- decay_rate: float32 [64, 64], P('tp'), may hold values from 0.05 to 2
- frequency: float32 [64, 64], P('tp'), may hold values from -3 to 3
- log_step: float32 [64], P('tp'), may hold values from -3 to 0.5
- b_real: float32 [64, 64, 16], P('tp'), may hold values from -1.5 to 1.5
- b_imag: float32 [64, 64, 16], P('tp'), may hold values from -1.5 to 1.5
- c_real: float32 [64, 16, 64], P('tp'), may hold values from -0.75 to 0.75
- c_imag: float32 [64, 16, 64], P('tp'), may hold values from -0.75 to 0.75
- skip_gain: float32 [1024], P('tp'), may hold values from -5 to 5
- states: float32 [2, 3072, 4096], P(None, 'ep', 'tp'), may hold values from -6 to 6
- out_proj: bfloat16 [1024, 4096], P('tp'), may hold values from -0.1875 to 0.1875
- route_ids: int32 [3072, 2], P('ep'), may hold values from 0 to 31, all different within a row; in each aligned block of 96 rows (0 to 95, 96 to 191, ...) at most 12 rows name the same one
- route_logits: float32 [3072, 2], P('ep'), may hold values from -5 to 5
- expert_gate: bfloat16 [32, 4096, 3072], P('ep', None, 'tp'), may hold values from -0.09375 to 0.09375
- expert_up: bfloat16 [32, 4096, 3072], P('ep', None, 'tp'), may hold values from -0.09375 to 0.09375
- expert_down: bfloat16 [32, 3072, 4096], P('ep', 'tp'), may hold values from -0.109375 to 0.109375
- dense_gate: bfloat16 [4096, 6144], P('tp', 'ep'), may hold values from -0.09375 to 0.09375
- dense_up: bfloat16 [4096, 6144], P('tp', 'ep'), may hold values from -0.09375 to 0.09375
- dense_down: bfloat16 [6144, 4096], P('ep', 'tp'), may hold values from -0.078125 to 0.078125
- branch_gate: bfloat16 [4096], replicated, may hold values from -0.09375 to 0.09375
Outputs:
- output: bfloat16 [3072, 4096], P('ep', 'tp')
- new_states: float32 [2, 3072, 4096], P(None, 'ep', 'tp')
Inputs may be any that keep to these rules, and one draw needn't show every extreme that they name: `route_ids`: each row names 2 different experts; among the rows of one device (aligned blocks of 96 rows) no expert is named by more than 12 rows.
All inputs are finite; a program needn't handle non-finite values.
Results may differ from a plain program's by a relative error of at most 0.017.
Values may be sent and summed in bfloat16 or wider, within the bound.
A program may use at most 128 MiB of HBM per device.

v0:
```python
import jax
import jax.numpy as jnp
from jax import lax
from jax.sharding import Mesh
from jax.sharding import PartitionSpec as P

GROUP = 16
STATE = 64
EP = ("ep_0", "ep_1")


def split_up(x, dim, peers):
    before, after = (x.shape[:dim], x.shape[dim + 1 :])
    return jnp.moveaxis(x.reshape(*before, peers, -1, *after), dim, 0)


def sent_and_summed(x, axis, dim):
    peers = lax.axis_size(axis)
    tiles = lax.all_to_all(split_up(x, dim, peers), axis, 0, 0, tiled=True)
    return jnp.sum(tiles.astype(jnp.float32), axis=0)


def sent_to_all(x, axis):
    peers = lax.axis_size(axis)
    return lax.all_to_all(jnp.broadcast_to(x[None], (peers, *x.shape)), axis, 0, 0, tiled=True)


def of_everyone(x, axis):
    return sent_to_all(x, axis).astype(jnp.float32).sum(axis=0)


def whole_of(x, axes, dim):
    for axis in reversed(axes):
        x = lax.all_gather(x, axis, axis=dim, tiled=True)
    return x


def rms_norm(values, gain):
    flt = values.astype(jnp.float32)
    scaled = flt * lax.rsqrt(jnp.mean(flt * flt, axis=-1, keepdims=True) + 1e-06)
    return (scaled * gain).astype(jnp.bfloat16)


def discretize(decay_rate, frequency, log_step, b_real, b_imag):
    step_size = jnp.exp(log_step)[:, None]
    lam_re = -decay_rate
    magnitude = jnp.exp(lam_re * step_size)
    abar_re = magnitude * jnp.cos(frequency * step_size)
    abar_im = magnitude * jnp.sin(frequency * step_size)
    denom = lam_re * lam_re + frequency * frequency
    fac_re = ((abar_re - 1.0) * lam_re + abar_im * frequency) / denom
    fac_im = (abar_im * lam_re - (abar_re - 1.0) * frequency) / denom
    bbar_re = fac_re[..., None] * b_real - fac_im[..., None] * b_imag
    bbar_im = fac_re[..., None] * b_imag + fac_im[..., None] * b_real
    return (abar_re, abar_im, bbar_re, bbar_im)


def state_step(
    drive, states, decay_rate, frequency, log_step, b_real, b_imag, c_real, c_imag, skip_gain
):
    count = drive.shape[0]
    groups = decay_rate.shape[0]
    abar_re, abar_im, bbar_re, bbar_im = discretize(decay_rate, frequency, log_step, b_real, b_imag)
    grouped = drive.astype(jnp.float32).reshape(count, groups, GROUP)
    old_re = states[0].reshape(count, groups, STATE)
    old_im = states[1].reshape(count, groups, STATE)
    push_re = jnp.einsum("ngh,gph->ngp", grouped, bbar_re)
    push_im = jnp.einsum("ngh,gph->ngp", grouped, bbar_im)
    new_re = abar_re * old_re - abar_im * old_im + push_re
    new_im = abar_re * old_im + abar_im * old_re + push_im
    readout = (
        jnp.einsum("ngp,ghp->ngh", new_re, c_real)
        - jnp.einsum("ngp,ghp->ngh", new_im, c_imag)
        + skip_gain.reshape(groups, GROUP) * grouped
    )
    reads = jax.nn.gelu(readout.reshape(count, groups * GROUP)).astype(jnp.bfloat16)
    fresh = jnp.stack(
        [new_re.reshape(count, groups * STATE), new_im.reshape(count, groups * STATE)]
    )
    return (reads, fresh)


def expert_rows(full_rows, gate_w, up_w, down_w, part_width):
    sources, items, width = full_rows.shape
    flat_rows = full_rows.reshape(sources * items, width)
    gate_val = jnp.dot(flat_rows, gate_w, preferred_element_type=jnp.float32)
    up_val = jnp.dot(flat_rows, up_w, preferred_element_type=jnp.float32)
    hidden = (jax.nn.silu(gate_val) * up_val).astype(jnp.bfloat16)
    partial_value = (
        jnp.dot(hidden, down_w, preferred_element_type=jnp.float32)
        .astype(jnp.bfloat16)
        .astype(jnp.float32)
    )
    summed = sent_and_summed(partial_value.astype(jnp.bfloat16), "tp", 1)
    return summed.astype(jnp.bfloat16).reshape(sources, items, part_width)


def shards(
    tokens,
    mix_gain,
    ffn_gain,
    in_proj,
    decay_rate,
    frequency,
    log_step,
    b_real,
    b_imag,
    c_real,
    c_imag,
    skip_gain,
    states,
    out_proj,
    route_ids,
    route_logits,
    expert_gate,
    expert_up,
    expert_down,
    dense_gate,
    dense_up,
    dense_down,
    branch_gate,
):
    seq_count, width = tokens.shape
    tp_count = lax.axis_size("tp")
    ep_count = lax.axis_size(EP)
    tp_index = lax.axis_index("tp")
    part_width = width // tp_count
    normed = rms_norm(tokens, mix_gain)
    drive = jnp.dot(normed, in_proj, preferred_element_type=jnp.float32).astype(jnp.bfloat16)
    reads, new_states = state_step(
        drive, states, decay_rate, frequency, log_step, b_real, b_imag, c_real, c_imag, skip_gain
    )
    partial_value = (
        jnp.dot(reads, out_proj, preferred_element_type=jnp.float32)
        .astype(jnp.bfloat16)
        .astype(jnp.float32)
    )
    mixed = (
        of_everyone(partial_value.astype(jnp.bfloat16), "tp")
        .astype(jnp.float32)
        .astype(jnp.bfloat16)
    )
    resid = (tokens.astype(jnp.float32) + mixed.astype(jnp.float32)).astype(jnp.bfloat16)
    normed_two = rms_norm(resid, ffn_gain)
    own_cols = lax.dynamic_slice_in_dim(normed_two, tp_index * part_width, part_width, 1)
    hidden_width = dense_gate.shape[1]
    both_proj = jnp.concatenate([dense_gate, dense_up], axis=1)
    partial_wide = jnp.dot(
        own_cols,
        lax.all_gather(both_proj, EP, axis=1, tiled=True),
        preferred_element_type=jnp.float32,
    )
    summed_wide = lax.psum(partial_wide.astype(jnp.bfloat16), "tp").astype(jnp.float32)
    arranged = summed_wide.reshape(seq_count, ep_count, 2, hidden_width)
    gate_all = arranged[:, :, 0, :].reshape(seq_count, ep_count * hidden_width)
    up_all = arranged[:, :, 1, :].reshape(seq_count, ep_count * hidden_width)
    dense_hidden = (jax.nn.silu(gate_all) * up_all).astype(jnp.bfloat16)
    dense_term = jnp.dot(
        dense_hidden, whole_of(dense_down, EP, 0), preferred_element_type=jnp.float32
    )
    top_count = route_ids.shape[1]
    capacity = max(2, 2 * seq_count * top_count // ep_count)
    flat_ids = route_ids.reshape(-1)
    onehot = (flat_ids[:, None] == jnp.arange(ep_count, dtype=jnp.int32)[None, :]).astype(jnp.int32)
    rank = jnp.cumsum(onehot, axis=0) - onehot
    slot = jnp.sum(rank * onehot, axis=1)
    target = flat_ids * capacity + slot
    select = target[None, :] == jnp.arange(ep_count * capacity, dtype=jnp.int32)[:, None]
    select = jnp.any(select.reshape(ep_count * capacity, seq_count, top_count), axis=2).astype(
        jnp.bfloat16
    )
    send_rows = jnp.dot(select, normed_two, preferred_element_type=jnp.float32).astype(jnp.bfloat16)
    send_rows = send_rows.reshape(ep_count, capacity, width)
    send_part = lax.dynamic_slice_in_dim(send_rows, tp_index * part_width, part_width, 2)
    full_rows = lax.all_gather(
        lax.all_to_all(send_part, EP, split_axis=0, concat_axis=0, tiled=True),
        "tp",
        axis=2,
        tiled=True,
    )
    answered = expert_rows(full_rows, expert_gate[0], expert_up[0], expert_down[0], part_width)
    returned = lax.all_to_all(answered, EP, split_axis=0, concat_axis=0, tiled=True)
    picked_rows = returned.reshape(ep_count * capacity, part_width)[target]
    picked_rows = picked_rows.reshape(seq_count, top_count, part_width).astype(jnp.float32)
    route_weights = jax.nn.softmax(route_logits, axis=-1)
    routed = jnp.sum(route_weights[..., None] * picked_rows, axis=1)
    branch = jax.nn.sigmoid(jnp.dot(normed_two, branch_gate, preferred_element_type=jnp.float32))
    resid_cols = lax.dynamic_slice_in_dim(resid, tp_index * part_width, part_width, 1).astype(
        jnp.float32
    )
    output = (resid_cols + routed + branch[:, None] * dense_term).astype(jnp.bfloat16)
    return (output, new_states)


def solution(mesh):
    finer = Mesh(mesh.devices.reshape(8, 4, mesh.shape["tp"]), ("ep_0", "ep_1", "tp"))
    return jax.shard_map(
        shards,
        mesh=finer,
        in_specs=(
            P(EP, None),
            P(),
            P(),
            P(None, "tp"),
            P("tp", None),
            P("tp", None),
            P("tp"),
            P("tp", None, None),
            P("tp", None, None),
            P("tp", None, None),
            P("tp", None, None),
            P("tp"),
            P(None, EP, "tp"),
            P("tp", None),
            P(EP, None),
            P(EP, None),
            P(EP, None, "tp"),
            P(EP, None, "tp"),
            P(EP, "tp", None),
            P("tp", EP),
            P("tp", EP),
            P(EP, "tp"),
            P(),
        ),
        out_specs=(P(EP, "tp"), P(None, EP, "tp")),
        check_vma=False,
    )
```

profile of v0, /device:TPU:8, one launch (start us, length us, event | category | flops | bytes accessed | tf_op | source)
XLA Modules:
  0.0 358.5 jit_solution(7874108804764348277)
XLA Ops:
  7.3 1.9 pad_maximum_fusion
  9.2 0.7 exp.20
  9.9 1.1 fusion.70
  10.9 0.8 copy.55
  11.8 0.8 copy.56
  12.6 1.4 fusion.8
  14.0 1.9 convolution_convert_fusion.4
  16.3 1.4 fusion.20
  17.7 1.0 fusion.71
  18.7 1.4 fusion.19
  20.1 1.1 fusion.25
  21.6 3.4 broadcast_in_dim.2
  25.0 7.0 %all-to-all-start = ((bf16[8,96,4096]{2,1,0:T(8,128)(2,1)}), bf16[8,96,4096]{2,1,0:T(8,128)(2,1)}, u32[]{:S(2)}, u32[]{:S(2)}) async-start(bf16[8,96,4096]{2,1,0:T(8,128)(2,1)} %broadcast_in_dim.2), calls=%async_computation | async-start | bytes 12582912 | tf_op jit(solution)/shard_map/all_to_all | solution.py:25
  32.2 0.6 reduce-window.6
  33.2 0.6 copy-done.9
  33.8 0.8 reduce_sum.77
  34.5 0.8 broadcast_multiply_fusion
  35.5 67.2 %all-to-all-done = bf16[8,96,4096]{2,1,0:T(8,128)(2,1)} async-done(((bf16[8,96,4096]{2,1,0:T(8,128)(2,1)}), bf16[8,96,4096]{2,1,0:T(8,128)(2,1)}, u32[]{:S(2)}, u32[]{:S(2)}) %all-to-all-start) | async-done | bytes 6291488 | tf_op jit(solution)/shard_map/all_to_all | solution.py:25
  102.7 5.2 %reduce_sum.74 = bf16[96,4096]{1,0:T(8,128)(2,1)} reduce(bf16[8,96,4096]{2,1,0:T(8,128)(2,1)} %all-to-all-done, bf16[]{:T(256)} %constant.14.clone.1), dimensions={0}, to_apply=%region_1.0 | reduce | flops 2752512 | bytes 7077890 | tf_op jit(solution)/shard_map/reduce_sum | solution.py:29
  108.0 1.8 fusion.5
  109.8 0.9 copy-done.4
  110.9 0.9 copy-done.2
  111.8 2.7 convolution_convert_fusion.1
  114.5 5.5 %reshape.129 = bf16[32,12,4096]{2,1,0:T(8,128)(2,1)} reshape(bf16[384,4096]{1,0:T(8,128)(2,1)} %convolution_convert_fusion.1) | data formatting | bytes 6291456 | tf_op jit(solution)/shard_map/reshape | solution.py:173
  120.0 1.1 constant_dynamic-slice_fusion
  121.0 26.9 %all_to_all.20 = bf16[32,12,512]{2,1,0:T(8,128)(2,1)} all-to-all(bf16[32,12,512]{2,1,0:T(8,128)(2,1)S(1)} %constant_dynamic-slice_fusion), channel_id=1, replica_groups=mesh['ep_0'=8,'ep_1'=4,'tp'=8] {'ep_0','ep_1'}, dimensions={0} | all-to-all | bytes 786432 | tf_op jit(solution)/shard_map/all_to_all | solution.py:176
  148.0 9.9 %convolution_convert_fusion = bf16[96,12288]{1,0:T(8,128)(2,1)} fusion(bf16[512,12288]{0,1:T(8,128)(2,1)} %all-gather.6.cloned.1.call-done, bf16[96,4096]{1,0:T(8,128)(2,1)} %copy-done.2, s32[]{:T(128)S(6)} %select_n.15), kind=kOutput, calls=%fused_computation.1 | convolution fusion | flops 1209139200 | bytes 15040516 | tf_op jit(solution)/shard_map/dot_general | solution.py:148
  158.0 6.2 %reshape.134 = bf16[96,32,2,192]{3,2,1,0:T(2,128)(2,1)} reshape(bf16[96,12288]{1,0:T(8,128)(2,1)} %convolution_convert_fusion) | data formatting | bytes 4718592 | tf_op jit(solution)/shard_map/reshape | solution.py:154
  164.2 15.9 %all_gather.14 = bf16[768,512]{1,0:T(8,128)(2,1)} all-gather(bf16[192,512]{1,0:T(8,128)(2,1)} %param.44), channel_id=1, replica_groups=mesh['ep_0'=8,'ep_1'=4,'tp'=8] {'ep_1'}, dimensions={0}, use_global_device_ids=true | all-gather | bytes 983040 | tf_op jit(solution)/shard_map/all_gather | solution.py:34
  180.1 5.6 %reshape.130 = bf16[384,4096]{1,0:T(8,128)(2,1)} reshape(bf16[32,12,4096]{2,1,0:T(8,128)(2,1)} %all-gather.4.cloned.1.call-done) | data formatting | bytes 6291456 | tf_op jit(solution)/shard_map/reshape | solution.py:85
  185.7 5.4 %fusion.3 = f32[384,384]{1,0:T(8,128)} fusion(bf16[384,4096]{1,0:T(8,128)(2,1)} %reshape.130, bf16[1,4096,384]{2,1,0:T(8,128)(2,1)} %param.39), kind=kOutput, calls=%fused_computation.11 | convolution fusion | flops 1207959552 | bytes 6881280 | tf_op jit(solution)/shard_map/dot_general | solution.py:86
  191.2 8.1 %convolution_convert_fusion.2 = bf16[384,4096]{1,0:T(8,128)(2,1)} fusion(bf16[1,384,4096]{2,1,0:T(8,128)(2,1)S(1)} %copy-done, bf16[384,4096]{1,0:T(8,128)(2,1)} %reshape.130, bf16[1,4096,384]{2,1,0:T(8,128)(2,1)} %param.40, f32[384,384]{1,0:T(8,128)} %fusion.3), kind=kOutput, calls=%fused_computation.3 | convolution fusion | flops 2418376704 | bytes 13172736 | tf_op jit(solution)/shard_map/dot_general | solution.py:90
  199.3 3.9 %copy.73 = bf16[48,8,8,512]{3,2,0,1:T(8,128)(2,1)} copy(bf16[48,8,8,512]{3,2,1,0:T(8,128)(2,1)} %bitcast.82) | data formatting | bytes 6291456 | tf_op jit(solution)/shard_map/reshape | solution.py:14
  203.2 4.9 %all-to-all-start.2 = ((bf16[8,384,512]{2,1,0:T(8,128)(2,1)}), bf16[8,384,512]{2,1,0:T(8,128)(2,1)S(1)}, u32[]{:S(2)}, u32[]{:S(2)}) async-start(bf16[8,384,512]{2,1,0:T(8,128)(2,1)} %bitcast.81), calls=%async_computation.2 | async-start | bytes 6291456 | tf_op jit(solution)/shard_map/all_to_all | solution.py:19
  208.2 40.3 %all-to-all-done.2 = bf16[8,384,512]{2,1,0:T(8,128)(2,1)S(1)} async-done(((bf16[8,384,512]{2,1,0:T(8,128)(2,1)}), bf16[8,384,512]{2,1,0:T(8,128)(2,1)S(1)}, u32[]{:S(2)}, u32[]{:S(2)}) %all-to-all-start.2) | async-done | bytes 3145760 | tf_op jit(solution)/shard_map/all_to_all | solution.py:19
  248.5 1.3 reduce_sum.79
  249.8 2.0 reshape.132
  251.8 9.2 %all-to-all-start.3 = ((bf16[32,12,512]{2,1,0:T(8,128)(2,1)}), bf16[32,12,512]{2,1,0:T(8,128)(2,1)S(1)}, u32[]{:S(2)}, u32[]{:S(2)}) async-start(bf16[32,12,512]{2,1,0:T(8,128)(2,1)} %reshape.132), calls=%async_computation.3 | async-start | bytes 1048576 | tf_op jit(solution)/shard_map/all_to_all | solution.py:182
  261.4 1.1 copy.66
  262.5 0.8 pad_maximum_fusion.1
  263.6 14.7 %all-to-all-done.3 = bf16[32,12,512]{2,1,0:T(8,128)(2,1)S(1)} async-done(((bf16[32,12,512]{2,1,0:T(8,128)(2,1)}), bf16[32,12,512]{2,1,0:T(8,128)(2,1)S(1)}, u32[]{:S(2)}, u32[]{:S(2)}) %all-to-all-start.3) | async-done | bytes 393248 | tf_op jit(solution)/shard_map/all_to_all | solution.py:182
  278.4 1.0 gather_fusion
  280.2 4.7 %reshape.135 = f32[96,32,2,192]{3,2,1,0:T(2,128)S(1)} convert(bf16[96,32,2,192]{3,2,1,0:T(2,128)(2,1)} %all-reduce.3.cloned.1.call-done) | non-fusion elementwise | flops 1179648 | bytes 7077888 | tf_op jit(solution)/shard_map/reshape | solution.py:154
  285.0 19.0 %slice_reduce_fusion.1 = (f32[96,32,192]{2,1,0:T(8,128)}, f32[96,32,192]{2,1,0:T(8,128)S(1)}) fusion(f32[96,32,2,192]{3,2,1,0:T(2,128)S(1)} %reshape.135), kind=kLoop, calls=%fused_computation.7 | loop fusion | bytes 9437184 | tf_op jit(solution)/shard_map/slice | solution.py:155
  304.0 4.2 %reshape_squeeze.14 = f32[96,6144]{1,0:T(8,128)} reshape(f32[96,32,192]{2,1,0:T(8,128)} %get-tuple-element.2) | data formatting | bytes 4718592 | tf_op jit(solution)/shard_map/reshape;squeeze | solution.py:155
  308.2 2.3 reshape_squeeze.15
  310.5 35.3 %all-gather.8.cloned.1.call-done = bf16[6144,512]{1,0:T(8,128)(2,1)} async-done(((bf16[768,512]{1,0:T(8,128)(2,1)}), bf16[6144,512]{1,0:T(8,128)(2,1)}) %all-gather.8.cloned.1.call-update) | async-done | bytes 6291472 | tf_op jit(solution)/shard_map/all_gather | solution.py:34
  345.8 6.1 %fusion.23 = bf16[96,512]{1,0:T(8,128)(2,1)} fusion(bf16[6144,512]{1,0:T(8,128)(2,1)} %all-gather.8.cloned.1.call-done, f32[96,6144]{1,0:T(8,128)} %reshape_squeeze.15, f32[96,6144]{1,0:T(8,128)} %reshape_squeeze.14, f32[96,512]{1,0:T(8,128)S(1)} %multiply_reduce_fusion, f32[96]{0:T(128)S(1)} %fusion.29, bf16[96,4096]{1,0:T(8,128)(2,1)} %copy-done.4, ...), kind=kOutput, calls=%fused_computation.35 | convolution fusion | flops 607764480 | bytes 11403652 | tf_op jit(solution)/shard_map/dot_general | solution.py:158
  (74 shorter events, 3.7 us)
Async XLA Ops:
  7.2 184.0 %copy-start = (bf16[1,384,4096]{2,1,0:T(8,128)(2,1)S(1)}, bf16[1,384,4096]{2,1,0:T(8,128)(2,1)}, u32[]{:S(2)}) copy-start(bf16[1,384,4096]{2,1,0:T(8,128)(2,1)} %param.41) | copy-start | bytes 9437188
  7.2 8.9 %copy-start.16 = (f32[128]{0:T(128)S(1)}, f32[128]{0:T(128)}, u32[]{:S(2)}) copy-start(f32[128]{0:T(128)} %param.34) | copy-start | bytes 1540
  7.2 9.0 %copy-start.14 = (f32[8,64]{1,0:T(8,128)S(1)}, f32[8,64]{1,0:T(8,128)}, u32[]{:S(2)}) copy-start(f32[8,64]{1,0:T(8,128)} %param.27) | copy-start | bytes 6148
  7.2 9.0 %copy-start.13 = (f32[8,64]{1,0:T(8,128)S(1)}, f32[8,64]{1,0:T(8,128)}, u32[]{:S(2)}) copy-start(f32[8,64]{1,0:T(8,128)} %param.28) | copy-start | bytes 6148
  7.2 140.8 %all-gather.6.cloned.1.call-start = ((), (), s32[]{:S(2)}) async-start(), calls=%async_computation.5 | async-start | bytes 12976128 | tf_op jit(solution)/shard_map/all_gather | solution.py:150
  11.8 4.5 %copy-start.7 = (f32[8,64,16]{1,2,0:T(8,128)S(1)}, f32[8,64,16]{1,2,0:T(8,128)}, u32[]{:S(2)}) copy-start(f32[8,64,16]{1,2,0:T(8,128)} %param.31) | copy-start | bytes 98308
  16.2 5.0 %copy-start.6 = (bf16[128,4096]{1,0:T(8,128)(2,1)S(1)}, bf16[128,4096]{1,0:T(8,128)(2,1)}, u32[]{:S(2)}) copy-start(bf16[128,4096]{1,0:T(8,128)(2,1)} %param.36) | copy-start | bytes 3145732
  20.1 1.1 copy-start.5
  25.0 7.0 %copy-start.15 = (s32[96,2]{0,1:T(2,128)S(1)}, s32[96,2]{0,1:T(2,128)}, u32[]{:S(2)}) copy-start(s32[96,2]{0,1:T(2,128)} %param.37) | copy-start | bytes 2308
  25.0 77.7 %all-to-all-start = ((bf16[8,96,4096]{2,1,0:T(8,128)(2,1)}), bf16[8,96,4096]{2,1,0:T(8,128)(2,1)}, u32[]{:S(2)}, u32[]{:S(2)}) async-start(bf16[8,96,4096]{2,1,0:T(8,128)(2,1)} %broadcast_in_dim.2), calls=%async_computation | async-start | bytes 12582912 | tf_op jit(solution)/shard_map/all_to_all | solution.py:25
  32.0 148.2 %all-gather.4.cloned.1.call-start = ((), (), s32[]{:S(2)}) async-start(), calls=%async_computation.4 | async-start | bytes 4718592 | tf_op jit(solution)/shard_map/all_gather | solution.py:175
  33.2 0.6 copy-start.9
  35.5 75.1 %copy-start.8 = (f32[4096]{0:T(1024)S(1)}, f32[4096]{0:T(1024)}, u32[]{:S(2)}) copy-start(f32[4096]{0:T(1024)} %param.25) | copy-start | bytes 49156
  109.7 0.9 copy-start.4
  110.9 0.9 copy-start.2
  148.0 132.3 %all-reduce.3.cloned.1.call-start = ((), (), s32[]{:S(2)}) async-start(), calls=%async_computation.6 | async-start | bytes 6291456 | tf_op jit(solution)/shard_map/psum | solution.py:153
  164.2 181.7 %all-gather.8.cloned.1.call-start = ((), (), s32[]{:S(2)}) async-start(), calls=%async_computation.7 | async-start | bytes 7077888 | tf_op jit(solution)/shard_map/all_gather | solution.py:34
  203.2 4.9 %copy-start.11 = (f32[96,2]{0,1:T(2,128)S(1)}, f32[96,2]{0,1:T(2,128)}, u32[]{:S(2)}) copy-start(f32[96,2]{0,1:T(2,128)} %param.38) | copy-start | bytes 2308
  203.2 45.3 %all-to-all-start.2 = ((bf16[8,384,512]{2,1,0:T(8,128)(2,1)}), bf16[8,384,512]{2,1,0:T(8,128)(2,1)S(1)}, u32[]{:S(2)}, u32[]{:S(2)}) async-start(bf16[8,384,512]{2,1,0:T(8,128)(2,1)} %bitcast.81), calls=%async_computation.2 | async-start | bytes 6291456 | tf_op jit(solution)/shard_map/all_to_all | solution.py:19
  208.2 53.1 %copy-start.12 = (bf16[4096]{0:T(1024)(128)(2,1)S(1)}, bf16[4096]{0:T(1024)(128)(2,1)}, u32[]{:S(2)}) copy-start(bf16[4096]{0:T(1024)(128)(2,1)} %param.45) | copy-start | bytes 24580
  208.2 54.3 %copy-start.10 = (s32[192]{0:T(256)S(1)}, s32[192]{0:T(256)}, u32[]{:S(2)}) copy-start(s32[192]{0:T(256)} %copy-done.9) | copy-start | bytes 2308
  249.8 13.5 %copy-start.3 = (bf16[96,4096]{1,0:T(8,128)(2,1)S(1)}, bf16[96,4096]{1,0:T(8,128)(2,1)}, u32[]{:S(2)}) copy-start(bf16[96,4096]{1,0:T(8,128)(2,1)} %copy-done.2) | copy-start | bytes 2359300
  251.8 26.5 %all-to-all-start.3 = ((bf16[32,12,512]{2,1,0:T(8,128)(2,1)}), bf16[32,12,512]{2,1,0:T(8,128)(2,1)S(1)}, u32[]{:S(2)}, u32[]{:S(2)}) async-start(bf16[32,12,512]{2,1,0:T(8,128)(2,1)} %reshape.132), calls=%async_computation.3 | async-start | bytes 1048576 | tf_op jit(solution)/shard_map/all_to_all | solution.py:182
  345.8 6.1 %copy-start.1 = (bf16[1,384,4096]{2,1,0:T(8,128)(2,1)S(1)}, bf16[1,384,4096]{2,1,0:T(8,128)(2,1)}, u32[]{:S(2)}) copy-start(bf16[1,384,4096]{2,1,0:T(8,128)(2,1)} %param.41) | copy-start | bytes 9437188
Sparse Core Ops, SparseCore 0:
  11.2 121.6 all-gather.5
  148.1 28.9 all-gather.3
  179.5 88.8 all-reduce.2
  270.0 75.7 all-gather.7
where the time goes:
time: 361 us; the launch traced here: 358 us
  waiting for transfers between devices  158 us (44%)
  local copies, waits for them, and re-layouts  63.2 us (18%)
  blocking collectives  42.7 us (12%)
  matrix products  39.8 us (11%)
  starting transfers between devices  21.2 us (6%)
  other arithmetic  19.8 us (5%)
  between operations  14.1 us (4%)
    all_to_all x1, waiting for transfers between devices, sent_to_all(): lax.all_to_all(jnp.broadcast_to(x[None], (peers, *x.shape)), axis, 0, 0,...  67.2 us
    all_to_all x1, waiting for transfers between devices, sent_and_summed(): tiles = lax.all_to_all(split_up(x, dim, peers), axis, 0, 0, tiled=True)  40.3 us
    all_gather x1, waiting for transfers between devices, whole_of(): x = lax.all_gather(x, axis, axis=dim, tiled=True)  35.3 us
    all_to_all x1, blocking collectives, shards(): lax.all_to_all(send_part, EP, split_axis=0, concat_axis=0, tiled=True)  26.9 us
    slice x1, local copies, waits for them, and re-layouts, shards(): gate_all = arranged[:, :, 0, :].reshape(seq_count, ep_count * hidden_width)  19 us
    all_gather x1, blocking collectives, whole_of(): x = lax.all_gather(x, axis, axis=dim, tiled=True)  15.9 us
    all_to_all x1, waiting for transfers between devices, shards(): lax.all_to_all(answered, EP, split_axis=0, concat_axis=0, tiled=True)  14.7 us
    dot_general x1, matrix products, shards(): jnp.dot(own_cols, lax.all_gather(both_proj, EP, axis=1, tiled=True), pref...  9.94 us
  transfers between devices with their start and end apart: 7, of which 4 were waited for; matrix products, arithmetic and copies ran while one was open for 31% of the time, Pallas kernels for 0%

commit v1 on v0

v1 whole, which is shorter than its diff:
```python
import functools
import heapq

import jax
import jax.numpy as jnp
from jax import lax
from jax.experimental import pallas as pl
from jax.experimental.pallas import tpu as pltpu
from jax.sharding import Mesh
from jax.sharding import PartitionSpec as P

GROUP = 16
STATE = 64
EP = ("ep_0", "ep_1")
MESH = pl.DeviceIdType.MESH


class Node:
    def __init__(self, chunk, off, parent, move):
        self.chunk, self.off, self.parent, self.move = chunk, off, parent, move
        self.kids = []
        if parent is not None:
            parent.kids.append(self)


def ring_offsets(size, far_up):
    up = size // 2 if far_up else (size - 1) // 2
    return up, size - 1 - up


def chain(chunk, root, axis, name, size, far_up):
    up, down = ring_offsets(size, far_up)
    found = [root]
    for step, count in ((1, up), (-1, down)) if far_up else ((-1, down), (1, up)):
        last = root
        for _ in range(count):
            off = list(last.off)
            off[axis] += step
            last = Node(chunk, tuple(off), last, (name, step))
            found.append(last)
    return found


def ep_tree(sizes):
    nodes = []
    for chunk in range(2):
        first, second = (0, 1) if chunk == 0 else (1, 0)
        root = Node(chunk, (0, 0), None, None)
        line = chain(chunk, root, first, EP[first], sizes[first], True)
        for i, node in enumerate(line):
            nodes += chain(chunk, node, second, EP[second], sizes[second], i % 2 == 0)
    return nodes


def tp_tree(tp_count, chunks):
    nodes = []
    for chunk in range(chunks):
        root = Node(chunk, (0, 0), None, None)
        line = chain(chunk, root, 0, "y", tp_count // 2, chunk % 2 == 0)
        for node in line:
            nodes += [node, Node(chunk, (node.off[0], 1), node, ("core", 1))]
    return nodes


def timed(nodes, cost, lag):
    free, heap, order = {}, [], []
    for i, node in enumerate(nodes):
        if node.parent is None:
            node.sent, node.came = 0.0, 0.0
            heapq.heappush(heap, (0.0, i))
    place = {id(node): i for i, node in enumerate(nodes)}
    while heap:
        now, i = heapq.heappop(heap)
        node = nodes[i]
        order.append(node)
        for kid in node.kids:
            price = cost * (0.35 if kid.move[0] == "core" else 1.0)
            start = max(now, free.get(kid.move, 0.0))
            free[kid.move] = start + price
            kid.sent, kid.came = start, start + price + lag
            heapq.heappush(heap, (kid.came, place[id(kid)]))
    for i, node in enumerate(order):
        node.index = i
    return order


class Places:
    def __init__(self, kind, sizes):
        self.kind, self.sizes = kind, sizes
        if kind == "ep":
            self.me = (lax.axis_index("ep_0"), lax.axis_index("ep_1"))
        else:
            t = lax.axis_index("tp")
            self.me = (t // 2, t % 2)

    def shifted(self, off):
        return tuple(
            lax.rem(m + (o + s), s) for m, o, s in zip(self.me, off, self.sizes)
        )

    def flat(self, at):
        return at[0] * self.sizes[1] + at[1]

    def owner(self, off, sign=-1):
        return self.flat(self.shifted(tuple(sign * o for o in off)))

    def device(self, move, sign=1):
        name, step = move
        step = step * sign
        if self.kind == "ep":
            axis = EP.index(name)
            return {name: lax.rem(self.me[axis] + (step + self.sizes[axis]), self.sizes[axis])}
        off = (step, 0) if name == "y" else (0, step)
        return {"tp": self.flat(self.shifted(off))}

    def greet(self):
        barrier = pltpu.get_barrier_semaphore()
        moves = [("ep_0", 1), ("ep_0", -1), ("ep_1", 1), ("ep_1", -1)]
        if self.kind == "tp":
            moves = [("y", 1), ("y", -1), ("core", 1)]
        for move in moves:
            pl.semaphore_signal(barrier, inc=1, device_id=self.device(move), device_id_type=MESH)
        pl.semaphore_wait(barrier, len(moves))


def gather_events(order, places, source, target, send, recv, events, base=0.0):
    started = []

    def copy(node, src, device):
        own = places.owner(node.parent.off) if node.parent is not None else None
        return pltpu.make_async_remote_copy(
            src_ref=src,
            dst_ref=target(node.chunk, own),
            send_sem=send.at[node.index],
            recv_sem=recv.at[node.index],
            device_id=device,
            device_id_type=MESH,
        )

    def handle(node):
        if node.parent is None:
            src = source(node.chunk)
        else:
            src = target(node.chunk, places.owner(node.off))
            pltpu.make_async_remote_copy(
                src_ref=src,
                dst_ref=src,
                send_sem=send.at[node.index],
                recv_sem=recv.at[node.index],
                device_id=places.device(node.move),
                device_id_type=MESH,
            ).wait_recv()
        for kid in node.kids:
            moved = copy(kid, src, places.device(kid.move))
            moved.start()
            started.append(moved)

    for node in order:
        events.append((base + node.came, functools.partial(handle, node)))
    return started


def add_into(out, terms, rows, step=16):
    def body(i, _):
        at = pl.ds(pl.multiple_of(i * step, step), step)
        total = terms[0](at).astype(jnp.float32)
        for term in terms[1:]:
            total = total + term(at).astype(jnp.float32)
        out(at, total)
        return 0

    lax.fori_loop(0, rows // step, body, 0)


def reduce_events(order, places, view, load, put, slots, sums, rows, send, recv, events, base=0.0):
    started = []
    last = max(node.came for node in order)

    def handle(node):
        off = node.off
        own = places.owner(off)
        for kid in node.kids:
            slot = slots.at[kid.index]
            pltpu.make_async_remote_copy(
                src_ref=slot,
                dst_ref=slot,
                send_sem=send.at[kid.index],
                recv_sem=recv.at[kid.index],
                device_id=places.device(kid.move),
                device_id_type=MESH,
            ).wait_recv()
        terms = [lambda at: load(node.chunk, own, at)]
        for kid in node.kids:
            terms.append(lambda at, k=kid.index: slots[k, at, :])
        if node.parent is None:
            add_into(lambda at, v: put(node.chunk, at, v), terms, rows)
            return
        if node.kids:
            src = sums.at[node.index]

            def keep(at, v):
                sums[node.index, at, :] = v.astype(sums.dtype)

            add_into(keep, terms, rows)
        else:
            src = view(node.chunk, own)
        moved = pltpu.make_async_remote_copy(
            src_ref=src,
            dst_ref=slots.at[node.index],
            send_sem=send.at[node.index],
            recv_sem=recv.at[node.index],
            device_id=places.device(node.move, -1),
            device_id_type=MESH,
        )
        moved.start()
        started.append(moved)

    for node in reversed(order):
        events.append((base + last - node.came, functools.partial(handle, node)))
    return started


def run_events(events, started):
    for _, act in sorted(events, key=lambda pair: pair[0]):
        act()
    for group in started:
        for moved in group:
            moved.wait_send()


def vmem(count):
    return [pl.BlockSpec(memory_space=pltpu.VMEM)] * count


def dma_sems(order):
    return [pltpu.SemaphoreType.DMA((len(order),))] * 2


def params(collective_id):
    return pltpu.CompilerParams(collective_id=collective_id, has_side_effects=True)


def mix_kernel(
    tp_count, width, reads, weights, tokens, gain, gate, route,
    normed, resid, branch, held, stats, send, recv, send2, recv2,
):
    me = lax.axis_index("tp")
    barrier = pltpu.get_barrier_semaphore()
    others = [lax.rem(me + k, tp_count) for k in range(1, tp_count)]
    for other in others:
        pl.semaphore_signal(barrier, inc=1, device_id={"tp": other}, device_id_type=MESH)
    pl.semaphore_wait(barrier, tp_count - 1)

    def exchange(src, dst, send, recv):
        copies = []
        for k, other in enumerate(others):
            copies.append(
                pltpu.make_async_remote_copy(
                    src_ref=src,
                    dst_ref=dst.at[k + 1],
                    send_sem=send.at[k],
                    recv_sem=recv.at[k],
                    device_id={"tp": other},
                    device_id_type=MESH,
                )
            )
            copies[-1].start()
        return copies

    copies = exchange(reads, held, send, recv)
    depth = reads.shape[1]
    f32 = jnp.float32

    def part(value, k):
        owner = lax.rem(me + tp_count - k, tp_count)
        at = pl.ds(pl.multiple_of(owner * depth, depth), depth)
        return jnp.dot(value, weights[at, :], preferred_element_type=f32)

    total = part(reads[...], 0)
    for k, copy in enumerate(copies):
        copy.wait()
        total = total + part(held[k + 1], k + 1)
    flt = tokens[...].astype(f32) + total.astype(jnp.bfloat16).astype(f32)
    flt = flt.astype(jnp.bfloat16).astype(f32)
    resid[...] = flt.astype(jnp.bfloat16)
    gained = flt * gain[...]
    ones = jnp.ones((8, flt.shape[1]), f32)
    high = lax.Precision.HIGHEST
    turned = (((1,), (1,)), ((), ()))
    square = lax.dot_general(ones, flt * flt, turned, precision=high, preferred_element_type=f32)
    logit = lax.dot_general(
        ones, gained * gate[...], turned, precision=high, preferred_element_type=f32
    )
    rows = flt.shape[0]
    stats[0, 0, :, :rows] = square
    stats[0, 1, :, :rows] = logit
    copies = exchange(stats.at[0], stats, send2, recv2)
    for copy in copies:
        copy.wait()
    both = stats[0]
    for k in range(1, tp_count):
        both = both + stats[k]
    scale = lax.rsqrt(both[0, :, :rows] / width + 1e-06)
    branch[...] = route[...]
    branch[:1, :rows] = jax.nn.sigmoid(scale * both[1, :, :rows])[:1]
    first = (lax.broadcasted_iota(jnp.int32, (8, flt.shape[1]), 0) == 0).astype(f32)
    column = lax.dot_general(
        scale, first, (((0,), (0,)), ((), ())), precision=high, preferred_element_type=f32
    )
    value = (gained * column).astype(jnp.bfloat16)
    half = rows // 2
    normed[0] = value[:half]
    normed[1] = value[half:]


def mix(reads, weights, tokens, gain, gate, route, tp_count, width):
    rows, cols = tokens.shape
    bf16, f32 = jnp.bfloat16, jnp.float32
    return pl.pallas_call(
        functools.partial(mix_kernel, tp_count, width),
        out_shape=(
            jax.ShapeDtypeStruct((2, rows // 2, cols), bf16),
            jax.ShapeDtypeStruct((rows, cols), bf16),
            jax.ShapeDtypeStruct((8, 128), f32),
        ),
        in_specs=vmem(6),
        out_specs=tuple(vmem(3)),
        scratch_shapes=[
            pltpu.VMEM((tp_count, *reads.shape), bf16),
            pltpu.VMEM((tp_count, 2, 8, 128), f32),
        ]
        + [pltpu.SemaphoreType.DMA((tp_count - 1,))] * 4,
        compiler_params=params(1),
        name="mix",
    )(reads, weights, tokens, gain, gate, route)


def spread_kernel(order, small, sizes, block, extra, out, out_extra, send, recv, send2, recv2):
    places = Places("ep", sizes)
    places.greet()
    mine = places.flat(places.me)
    events = []
    one = gather_events(
        order, places, lambda c: block.at[c], lambda c, b: out.at[b, c], send, recv, events
    )
    two = gather_events(
        small, places, lambda c: extra, lambda c, b: out_extra.at[b], send2, recv2, events, 0.1
    )
    out[mine] = block[...]
    out_extra[mine] = extra[...]
    run_events(events, (one, two))


def spread(block, extra, sizes):
    count = sizes[0] * sizes[1]
    order = timed(ep_tree(sizes), 1.0, 1.8)
    small = timed([n for n in ep_tree(sizes) if n.chunk == 0], 0.1, 1.8)
    return pl.pallas_call(
        functools.partial(spread_kernel, order, small, sizes),
        out_shape=(
            jax.ShapeDtypeStruct((count, *block.shape), block.dtype),
            jax.ShapeDtypeStruct((count, *extra.shape), extra.dtype),
        ),
        in_specs=vmem(2),
        out_specs=tuple(vmem(2)),
        scratch_shapes=dma_sems(order) + dma_sems(small),
        compiler_params=params(2),
        name="spread",
    )(block, extra)


def expert_in_kernel(
    order, order2, order3, sizes, half, rows, wide,
    full, hid_all, mine, slots, sums, send, recv, send2, recv2, send3, recv3,
):
    places = Places("tp", sizes)
    places.greet()
    me = places.flat(places.me)
    part = rows.shape[2]
    span = rows.shape[1]
    events, f32 = [], jnp.float32

    def columns(b):
        return pl.ds(pl.multiple_of(b * part, part), part)

    def put(chunk, at, value):
        gate, up = value[:, :half], value[:, half:]
        hidden = gate * jax.nn.sigmoid(gate) * up
        mine[chunk, at, :] = hidden.astype(mine.dtype)

    count = wide.shape[2]
    one = reduce_events(
        order2, places,
        lambda c, b: wide.at[b, c], lambda c, b, at: wide[b, c, at, :], put,
        slots, sums, count, send2, recv2, events,
    )
    lastly = max(at for at, _ in events)
    two = gather_events(
        order, places, lambda c: rows.at[c],
        lambda c, b: full.at[pl.ds(c * span, span), columns(b)],
        send, recv, events, 0.01,
    )
    three = gather_events(
        order3, places, lambda c: mine.at[c], lambda c, b: hid_all.at[b, c],
        send3, recv3, events, lastly + 0.01,
    )
    for c in range(rows.shape[0]):
        full[pl.ds(c * span, span), columns(me)] = rows[c]
    run_events(events, (one, two, three))
    hid_all[me] = mine[...]


def expert_in(rows, wide, half, tp_count):
    sizes = (tp_count // 2, 2)
    order = timed(tp_tree(tp_count, 2), 4.2, 1.0)
    order2 = timed(tp_tree(tp_count, 2), 3.2, 1.0)
    order3 = timed(tp_tree(tp_count, 2), 1.6, 1.0)
    bf16 = rows.dtype
    chunks, span, part = rows.shape
    _, _, count, cols = wide.shape
    return pl.pallas_call(
        functools.partial(expert_in_kernel, order, order2, order3, sizes, half),
        out_shape=(
            jax.ShapeDtypeStruct((chunks * span, part * tp_count), bf16),
            jax.ShapeDtypeStruct((tp_count, 2, count, half), bf16),
        ),
        in_specs=vmem(2),
        out_specs=tuple(vmem(2)),
        scratch_shapes=[
            pltpu.VMEM((2, count, half), bf16),
            pltpu.VMEM((len(order2), count, cols), bf16),
            pltpu.VMEM((len(order2), count, cols), bf16),
        ]
        + dma_sems(order) + dma_sems(order2) + dma_sems(order3),
        compiler_params=params(3),
        name="expert_in",
    )(rows, wide)


def expert_out_kernel(order, sizes, partial, weight, out, slots, sums, send, recv):
    places = Places("tp", sizes)
    places.greet()
    chunks, span, part = out.shape
    events = []

    def columns(b):
        return pl.ds(pl.multiple_of(b * part, part), part)

    def load(c, b, at):
        return partial[c, at, columns(b)]

    def put(c, at, value):
        out[c, at, :] = (value * weight[c, at, :1]).astype(out.dtype)

    one = reduce_events(
        order, places, lambda c, b: partial.at[c, :, columns(b)], load, put,
        slots, sums, span, send, recv, events,
    )
    run_events(events, (one,))


def expert_out(partial, weight, tp_count):
    sizes = (tp_count // 2, 2)
    order = timed(tp_tree(tp_count, 2), 4.2, 1.0)
    chunks, span, width = partial.shape
    part = width // tp_count
    bf16 = partial.dtype
    return pl.pallas_call(
        functools.partial(expert_out_kernel, order, sizes),
        out_shape=jax.ShapeDtypeStruct((chunks, span, part), bf16),
        in_specs=vmem(2),
        out_specs=vmem(1)[0],
        scratch_shapes=[pltpu.VMEM((len(order), span, part), bf16)] * 2 + dma_sems(order),
        compiler_params=params(4),
        name="expert_out",
    )(partial, weight)


def collect_kernel(order, sizes, blocks, resid, out, slots, sums, send, recv):
    places = Places("ep", sizes)
    places.greet()
    events = []

    def put(c, at, value):
        out[c, at, :] = (resid[c, at, :].astype(jnp.float32) + value).astype(out.dtype)

    one = reduce_events(
        order, places, lambda c, b: blocks.at[b, c], lambda c, b, at: blocks[b, c, at, :], put,
        slots, sums, resid.shape[1], send, recv, events,
    )
    run_events(events, (one,))


def collect(blocks, resid, sizes):
    order = timed(ep_tree(sizes), 1.0, 1.8)
    _, _, rows, cols = blocks.shape
    bf16 = blocks.dtype
    return pl.pallas_call(
        functools.partial(collect_kernel, order, sizes),
        out_shape=jax.ShapeDtypeStruct(resid.shape, bf16),
        in_specs=vmem(2),
        out_specs=vmem(1)[0],
        scratch_shapes=[pltpu.VMEM((len(order), rows, cols), bf16)] * 2 + dma_sems(order),
        compiler_params=params(5),
        name="collect",
    )(blocks, resid)


def split_up(x, dim, peers):
    before, after = (x.shape[:dim], x.shape[dim + 1 :])
    return jnp.moveaxis(x.reshape(*before, peers, -1, *after), dim, 0)


def rms_norm(values, gain):
    flt = values.astype(jnp.float32)
    scaled = flt * lax.rsqrt(jnp.mean(flt * flt, axis=-1, keepdims=True) + 1e-06)
    return (scaled * gain).astype(jnp.bfloat16)


def discretize(decay_rate, frequency, log_step, b_real, b_imag):
    step_size = jnp.exp(log_step)[:, None]
    lam_re = -decay_rate
    magnitude = jnp.exp(lam_re * step_size)
    abar_re = magnitude * jnp.cos(frequency * step_size)
    abar_im = magnitude * jnp.sin(frequency * step_size)
    denom = lam_re * lam_re + frequency * frequency
    fac_re = ((abar_re - 1.0) * lam_re + abar_im * frequency) / denom
    fac_im = (abar_im * lam_re - (abar_re - 1.0) * frequency) / denom
    bbar_re = fac_re[..., None] * b_real - fac_im[..., None] * b_imag
    bbar_im = fac_re[..., None] * b_imag + fac_im[..., None] * b_real
    return (abar_re, abar_im, bbar_re, bbar_im)


def state_step(
    drive, states, decay_rate, frequency, log_step, b_real, b_imag, c_real, c_imag, skip_gain
):
    count = drive.shape[0]
    groups = decay_rate.shape[0]
    abar_re, abar_im, bbar_re, bbar_im = discretize(decay_rate, frequency, log_step, b_real, b_imag)
    grouped = drive.astype(jnp.float32).reshape(count, groups, GROUP)
    old_re = states[0].reshape(count, groups, STATE)
    old_im = states[1].reshape(count, groups, STATE)
    push_re = jnp.einsum("ngh,gph->ngp", grouped, bbar_re)
    push_im = jnp.einsum("ngh,gph->ngp", grouped, bbar_im)
    new_re = abar_re * old_re - abar_im * old_im + push_re
    new_im = abar_re * old_im + abar_im * old_re + push_im
    readout = (
        jnp.einsum("ngp,ghp->ngh", new_re, c_real)
        - jnp.einsum("ngp,ghp->ngh", new_im, c_imag)
        + skip_gain.reshape(groups, GROUP) * grouped
    )
    reads = jax.nn.gelu(readout.reshape(count, groups * GROUP)).astype(jnp.bfloat16)
    fresh = jnp.stack(
        [new_re.reshape(count, groups * STATE), new_im.reshape(count, groups * STATE)]
    )
    return (reads, fresh)


def shards(
    tokens,
    mix_gain,
    ffn_gain,
    in_proj,
    decay_rate,
    frequency,
    log_step,
    b_real,
    b_imag,
    c_real,
    c_imag,
    skip_gain,
    states,
    out_proj,
    route_ids,
    route_logits,
    expert_gate,
    expert_up,
    expert_down,
    dense_gate,
    dense_up,
    dense_down,
    branch_gate,
):
    seq_count, width = tokens.shape
    tp_count = lax.axis_size("tp")
    ep_count = lax.axis_size(EP)
    tp_index = lax.axis_index("tp")
    ep_index = lax.axis_index(EP)
    part_width = width // tp_count
    f32, bf16 = jnp.float32, jnp.bfloat16
    top_count = route_ids.shape[1]
    capacity = max(2, 2 * seq_count * top_count // ep_count)
    slots = ep_count * capacity

    route_weights = jax.nn.softmax(route_logits, axis=-1)
    route_rows = jnp.zeros((8, 128), f32)
    route_rows = route_rows.at[1 : 1 + top_count, :seq_count].set(route_ids.astype(f32).T)
    weight_at = 1 + top_count
    route_rows = route_rows.at[weight_at : weight_at + top_count, :seq_count].set(route_weights.T)

    out_cols = lax.all_to_all(split_up(out_proj, 1, tp_count), "tp", 0, 0, tiled=True)
    out_cols = out_cols.reshape(tp_count * out_proj.shape[0], part_width)

    normed = rms_norm(tokens, mix_gain)
    drive = jnp.dot(normed, in_proj, preferred_element_type=f32).astype(bf16)
    reads, new_states = state_step(
        drive, states, decay_rate, frequency, log_step, b_real, b_imag, c_real, c_imag, skip_gain
    )
    token_cols = lax.dynamic_slice_in_dim(tokens, tp_index * part_width, part_width, 1)
    gain_cols = lax.dynamic_slice_in_dim(ffn_gain, tp_index * part_width, part_width, 0)[None]
    gate_cols = lax.dynamic_slice_in_dim(branch_gate, tp_index * part_width, part_width, 0)
    normed_two, resid, branch = mix(
        reads, out_cols, token_cols, gain_cols, gate_cols.astype(f32)[None], route_rows,
        tp_count, width
    )
    sizes = (lax.axis_size("ep_0"), lax.axis_size("ep_1"))
    everyone, branch_all = spread(normed_two, branch, sizes)
    everyone = everyone.reshape(ep_count * seq_count, part_width)
    route_all = branch_all[:, 1:, :seq_count]
    match = (route_all[:, :top_count] == ep_index.astype(f32)).astype(f32)
    named = jnp.sum(match, axis=1)
    weight_all = jnp.sum(match * route_all[:, top_count : 2 * top_count], axis=1).reshape(-1)
    order = jnp.arange(seq_count)
    before = (order[:, None] < order[None, :]).astype(f32)
    slot = jnp.dot(named, before, preferred_element_type=f32)
    place = slot + capacity * jnp.arange(ep_count, dtype=f32)[:, None]
    place = jnp.where(named > 0, place, -1.0).reshape(-1)
    select = place[None, :] == jnp.arange(slots, dtype=f32)[:, None]
    select = select.astype(bf16)
    row_weight = jnp.sum(select.astype(f32) * weight_all[None, :], axis=1)
    branch_all = branch_all[:, 0, :seq_count].reshape(ep_count * seq_count, 1)

    both_proj = jnp.concatenate([dense_gate, dense_up], axis=1)
    hidden_width = dense_gate.shape[1]
    wide = jnp.dot(everyone, both_proj, preferred_element_type=f32).astype(bf16)
    rows_in = jnp.dot(select, everyone, preferred_element_type=f32).astype(bf16)
    full_rows, dense_hidden = expert_in(
        rows_in.reshape(2, slots // 2, part_width),
        wide.reshape(tp_count, 2, -1, 2 * hidden_width),
        hidden_width,
        tp_count,
    )
    dense_hidden = dense_hidden.reshape(ep_count * seq_count, hidden_width)
    gate_val = jnp.dot(full_rows, expert_gate[0], preferred_element_type=f32)
    up_val = jnp.dot(full_rows, expert_up[0], preferred_element_type=f32)
    hidden = (jax.nn.silu(gate_val) * up_val).astype(bf16)
    partial = jnp.dot(hidden, expert_down[0], preferred_element_type=f32).astype(bf16)
    row_weight = jnp.broadcast_to(row_weight[:, None], (slots, 128)).reshape(2, slots // 2, 128)
    weighted = expert_out(partial.reshape(2, slots // 2, width), row_weight, tp_count)
    weighted = weighted.reshape(slots, part_width)

    dense_part = jnp.dot(dense_hidden, dense_down, preferred_element_type=f32)
    routed = lax.dot_general(select, weighted, (((0,), (0,)), ((), ())), preferred_element_type=f32)
    mine = (routed + branch_all * dense_part).astype(bf16)
    output = collect(
        mine.reshape(ep_count, 2, seq_count // 2, part_width),
        resid.reshape(2, seq_count // 2, part_width),
        sizes,
    )
    return (output.reshape(seq_count, part_width), new_states)


def solution(mesh):
    finer = Mesh(mesh.devices.reshape(8, 4, mesh.shape["tp"]), ("ep_0", "ep_1", "tp"))
    return jax.shard_map(
        shards,
        mesh=finer,
        in_specs=(
            P(EP, None),
            P(),
            P(),
            P(None, "tp"),
            P("tp", None),
            P("tp", None),
            P("tp"),
            P("tp", None, None),
            P("tp", None, None),
            P("tp", None, None),
            P("tp", None, None),
            P("tp"),
            P(None, EP, "tp"),
            P("tp", None),
            P(EP, None),
            P(EP, None),
            P(EP, None, "tp"),
            P(EP, None, "tp"),
            P(EP, "tp", None),
            P("tp", EP),
            P("tp", EP),
            P(EP, "tp"),
            P(),
        ),
        out_specs=(P(EP, "tp"), P(None, EP, "tp")),
        check_vma=False,
    )
```

time: 361 us -> 225 us (0.62)
  waiting for transfers between devices: 158 us -> 0.01 us
  Pallas kernels: 0 us -> 156 us
  local copies, waits for them, and re-layouts: 63.2 us -> 17.5 us
  blocking collectives: 42.7 us -> 0 us
  starting transfers between devices: 21.2 us -> 6.41 us
  between operations: 14.1 us -> 0.92 us
  other arithmetic: 19.8 us -> 8.52 us
  matrix products: 39.8 us -> 34.1 us
    pallas_call x0 -> x5, Pallas kernels: none -> 156 us  [the longest x1 44.2 us: spread(): pl.pallas_call(functools.partial(spread_kernel, order, small, sizes), out...]
    all_to_all x3 -> x1, waiting for transfers between devices: 122 us -> 0.01 us  [shards(): lax.all_to_all(split_up(out_proj, 1, tp_count), 'tp', 0, 0, tiled=True)]
    all_gather x3 -> x0, waiting for transfers between devices: 35.3 us -> none  [the longest x1 35.3 us: whole_of(): x = lax.all_gather(x, axis, axis=dim, tiled=True)]
    all_to_all x1 -> x0, blocking collectives: 26.9 us -> none  [shards(): lax.all_to_all(send_part, EP, split_axis=0, concat_axis=0, tiled=True)]
    reshape x5 -> x1, local copies, waits for them, and re-layouts: 19.3 us -> 0.08 us  [state_step(): readout.reshape(count, groups * GROUP)]
    slice x2 -> x1, local copies, waits for them, and re-layouts: 19.2 us -> 0.95 us  [shards(): branch_all = branch_all[:, 0, :seq_count].reshape(ep_count * seq_count, 1)]
    all_gather x1 -> x0, blocking collectives: 15.9 us -> none  [whole_of(): x = lax.all_gather(x, axis, axis=dim, tiled=True)]
    all_to_all x3 -> x1, starting transfers between devices: 21 us -> 6.41 us  [shards(): lax.all_to_all(split_up(out_proj, 1, tp_count), 'tp', 0, 0, tiled=True)]
  transfers between devices with their start and end apart: 7 -> 1, of which waited for: 4 -> 0; matrix products, arithmetic and copies ran while one was open for 31% -> 11% of each run, Pallas kernels for 0% -> 0%
where the time goes in v1:
time: 225 us; the launch traced here: 224 us
  Pallas kernels  156 us (69%)
  matrix products  34.1 us (15%)
  local copies, waits for them, and re-layouts  17.5 us (8%)
  other arithmetic  8.52 us (4%)
  starting transfers between devices  6.41 us (3%)
    pallas_call x1, Pallas kernels, spread(): pl.pallas_call(functools.partial(spread_kernel, order, small, sizes), out...  44.2 us
    pallas_call x1, Pallas kernels, expert_in(): pl.pallas_call(functools.partial(expert_in_kernel, order, order2, order3,...  42.1 us
    pallas_call x1, Pallas kernels, collect(): pl.pallas_call(functools.partial(collect_kernel, order, sizes), out_shape...  34.2 us
    pallas_call x1, Pallas kernels, expert_out(): pl.pallas_call(functools.partial(expert_out_kernel, order, sizes), out_sh...  22.6 us
    pallas_call x1, Pallas kernels, mix(): pl.pallas_call(functools.partial(mix_kernel, tp_count, width), out_shape=...  13 us
    dot_general x1, matrix products, shards(): jnp.dot(hidden, expert_down[0], preferred_element_type=f32).astype(bf16)  8.06 us
    all_to_all x1, starting transfers between devices, shards(): lax.all_to_all(split_up(out_proj, 1, tp_count), 'tp', 0, 0, tiled=True)  6.41 us
    dot_general x1, matrix products, shards(): gate_val = jnp.dot(full_rows, expert_gate[0], preferred_element_type=f32)  5.5 us
  transfers between devices with their start and end apart: 1, of which 0 were waited for; matrix products, arithmetic and copies ran while one was open for 11% of the time, Pallas kernels for 0%

profile of v1, /device:TPU:8, one launch (start us, length us, event | category | flops | bytes accessed | tf_op | source)
XLA Modules:
  0.0 223.6 jit_solution(8109425001842564769)
XLA Ops:
  0.6 0.0 copy-start
  0.7 2.5 %copy.58 = bf16[16,8,8,512]{3,2,0,1:T(8,128)(2,1)} copy(bf16[16,8,8,512]{3,2,1,0:T(8,128)(2,1)} %bitcast.83) | data formatting | bytes 2097152 | tf_op jit(solution)/shard_map/reshape | solution.py:511
  3.2 6.4 %all-to-all-start = ((bf16[8,128,512]{2,1,0:T(8,128)(2,1)}), bf16[8,128,512]{2,1,0:T(8,128)(2,1)}, u32[]{:S(2)}, u32[]{:S(2)}) async-start(bf16[8,128,512]{2,1,0:T(8,128)(2,1)} %bitcast.72), calls=%async_computation | async-start | bytes 2097152 | tf_op jit(solution)/shard_map/all_to_all | solution.py:601
  9.6 1.4 fusion.10
  11.0 1.9 convolution_convert_fusion.2
  12.9 0.1 copy.47
  13.0 1.8 fusion.60
  14.9 1.0 copy.45
  15.9 1.9 copy.46
  17.8 0.1 add_divide_fusion
  17.9 2.0 fusion.20
  19.9 1.4 fusion.21
  21.3 0.6 convert_bitcast_fusion
  21.8 0.1 mul.225
  21.9 1.0 fusion.61
  22.9 1.1 fusion.23
  24.1 0.1 copy.52
  24.2 1.8 copy.55
  25.9 0.8 copy.54
  26.7 1.3 dynamic_slice.10
  28.1 0.7 scatter.6
  28.7 0.7 divide_bitcast_fusion
  29.4 0.3 scatter.9.route
  29.7 1.4 dynamic-slice_convert_fusion
  31.1 1.5 constant_dynamic-slice_fusion.tokens
  32.6 1.8 pad_maximum_fusion
  34.4 0.6 fusion.52.reads
  35.0 13.0 %mix.1 = (bf16[2,48,512]{2,1,0:T(8,128)(2,1)}, bf16[96,512]{1,0:T(8,128)(2,1)}, f32[8,128]{1,0:T(8,128)}) custom-call(bf16[96,128]{1,0:T(8,128)(2,1)} %fusion.52.reads, bf16[1024,512]{1,0:T(8,128)(2,1)} %bitcast.8.weights, bf16[96,512]{1,0:T(8,128)(2,1)} %constant_dynamic-slice_fusion.tokens, f32[1,512]{1,0:T(1,128)} %bitcast.92, f32[1,512]{1,0:T(1,128)} %bitcast.91, ...), custom_call_target="tpu_custom_call" | custom-call | tf_op jit(solution)/shard_map/mix/pallas_call | solution.py:319
  48.1 44.2 %spread.1 = (bf16[32,2,48,512]{3,2,1,0:T(8,128)(2,1)}, f32[32,8,128]{2,1,0:T(8,128)}) custom-call(bf16[2,48,512]{2,1,0:T(8,128)(2,1)} %get-tuple-element.33.block, f32[8,128]{1,0:T(8,128)} %get-tuple-element.34.extra), custom_call_target="tpu_custom_call" | custom-call | tf_op jit(solution)/shard_map/spread/pallas_call | solution.py:358
  92.3 0.9 slice_reduce_fusion
  93.2 1.1 select_reduce_fusion
  94.3 0.1 mul.245
  94.4 0.1 mul.242
  94.4 0.1 fusion.24
  94.5 0.1 eq.23
  94.6 0.8 multiply_reduce_fusion
  95.5 0.1 broadcast_in_dim.17
  95.5 4.2 %fusion.16 = bf16[384,512]{1,0:T(8,128)(2,1)} fusion(bf16[3072,512]{1,0:T(8,128)(2,1)} %bitcast.93, f32[3072]{0:T(1024)S(1)} %eq.23), kind=kOutput, calls=%fused_computation.21 | convolution fusion | flops 1209335808 | bytes 3551232 | tf_op jit(solution)/shard_map/dot_general | solution.py:636
  99.8 3.3 %convolution_convert_fusion.1 = bf16[3072,384]{1,0:T(8,128)(2,1)} fusion(bf16[3072,512]{1,0:T(8,128)(2,1)S(1)} %bitcast.94, bf16[512,192]{0,1:T(8,128)(2,1)S(1)} %copy-done.13, bf16[512,192]{0,1:T(8,128)(2,1)S(1)} %copy-done.14), kind=kOutput, calls=%fused_computation.7 | convolution fusion | flops 1209925632 | bytes 5898240 | tf_op jit(solution)/shard_map/dot_general | solution.py:635
  103.0 42.1 %expert_in.1 = (bf16[384,4096]{1,0:T(8,128)(2,1)}, bf16[8,2,192,192]{3,2,1,0:T(8,128)(2,1)}) custom-call(bf16[2,192,512]{2,1,0:T(8,128)(2,1)} %bitcast.88, bf16[8,2,192,384]{3,2,1,0:T(8,128)(2,1)} %bitcast.74), custom_call_target="tpu_custom_call" | custom-call | tf_op jit(solution)/shard_map/expert_in/pallas_call | solution.py:421
  145.1 5.5 %fusion.6 = f32[384,384]{1,0:T(8,128)} fusion(bf16[384,4096]{1,0:T(8,128)(2,1)} %get-tuple-element.37, bf16[1,4096,384]{2,1,0:T(8,128)(2,1)} %param.43), kind=kOutput, calls=%fused_computation.11 | convolution fusion | flops 1207959552 | bytes 6881280 | tf_op jit(solution)/shard_map/dot_general | solution.py:644
  150.6 8.1 %convolution_convert_fusion = bf16[384,4096]{1,0:T(8,128)(2,1)} fusion(bf16[1,384,4096]{2,1,0:T(8,128)(2,1)S(1)} %copy-done, bf16[384,4096]{1,0:T(8,128)(2,1)} %get-tuple-element.37, bf16[1,4096,384]{2,1,0:T(8,128)(2,1)} %param.44, f32[384,384]{1,0:T(8,128)} %fusion.6), kind=kOutput, calls=%fused_computation.1 | convolution fusion | flops 2418376704 | bytes 13172736 | tf_op jit(solution)/shard_map/dot_general | solution.py:647
  158.7 0.8 broadcast_in_dim.18.weight
  159.5 22.6 %expert_out.1 = bf16[2,192,512]{2,1,0:T(8,128)(2,1)} custom-call(bf16[2,192,4096]{2,1,0:T(8,128)(2,1)} %bitcast.73, f32[2,192,128]{2,1,0:T(8,128)} %broadcast_in_dim.18.weight), custom_call_target="tpu_custom_call" | custom-call | tf_op jit(solution)/shard_map/expert_out/pallas_call | solution.py:468
  182.2 3.0 %fusion = f32[3072,512]{1,0:T(8,128)S(1)} fusion(bf16[384,512]{1,0:T(8,128)(2,1)} %bitcast.82, f32[3072]{0:T(1024)S(1)} %eq.23), kind=kOutput, calls=%fused_computation.4 | convolution fusion | flops 1209139200 | bytes 6696960 | tf_op jit(solution)/shard_map/dot_general | solution.py:653
  185.2 2.7 %add_convert_fusion = bf16[3072,512]{1,0:T(8,128)(2,1)} fusion(f32[3072,512]{1,0:T(8,128)S(1)} %fusion, bf16[3072,192]{1,0:T(8,128)(2,1)S(1)} %bitcast.81, bf16[192,512]{1,0:T(8,128)(2,1)S(1)} %copy-done.4, f32[3072]{0:T(1024)S(1)} %mul.245), kind=kOutput, calls=%fused_computation | convolution fusion | flops 608698368 | bytes 10825728 | tf_op jit(solution)/shard_map/dot_general | solution.py:652
  187.9 34.2 %collect.1 = bf16[2,48,512]{2,1,0:T(8,128)(2,1)} custom-call(bf16[32,2,48,512]{3,2,1,0:T(8,128)(2,1)} %bitcast.71, bf16[2,48,512]{2,1,0:T(8,128)(2,1)} %bitcast.90), custom_call_target="tpu_custom_call" | custom-call | tf_op jit(solution)/shard_map/collect/pallas_call | solution.py:498
  222.1 1.5 copy.61
  (39 shorter events, 0.1 us)
Async XLA Ops:
  0.6 150.0 %copy-start = (bf16[1,384,4096]{2,1,0:T(8,128)(2,1)S(1)}, bf16[1,384,4096]{2,1,0:T(8,128)(2,1)}, u32[]{:S(2)}) copy-start(bf16[1,384,4096]{2,1,0:T(8,128)(2,1)} %param.45) | copy-start | bytes 9437188
  0.6 8.9 %copy-start.16 = (f32[8]{0:T(128)S(1)}, f32[8]{0:T(128)}, u32[]{:S(2)}) copy-start(f32[8]{0:T(128)} %param.33) | copy-start | bytes 100
  0.7 10.4 %copy-start.15 = (f32[4096]{0:T(1024)S(1)}, f32[4096]{0:T(1024)}, u32[]{:S(2)}) copy-start(f32[4096]{0:T(1024)} %param.28) | copy-start | bytes 49156
  3.2 14.6 %copy-start.8 = (f32[8,64]{1,0:T(8,128)S(1)}, f32[8,64]{1,0:T(8,128)}, u32[]{:S(2)}) copy-start(f32[8,64]{1,0:T(8,128)} %param.32) | copy-start | bytes 6148
  3.2 14.6 %copy-start.9 = (f32[8,64]{1,0:T(8,128)S(1)}, f32[8,64]{1,0:T(8,128)}, u32[]{:S(2)}) copy-start(f32[8,64]{1,0:T(8,128)} %param.31) | copy-start | bytes 6148
  3.2 14.8 %copy-start.3 = (f32[8,64,16]{1,2,0:T(8,128)S(1)}, f32[8,64,16]{1,2,0:T(8,128)}, u32[]{:S(2)}) copy-start(f32[8,64,16]{1,2,0:T(8,128)} %param.35) | copy-start | bytes 98308
  3.2 31.9 %all-to-all-start = ((bf16[8,128,512]{2,1,0:T(8,128)(2,1)}), bf16[8,128,512]{2,1,0:T(8,128)(2,1)}, u32[]{:S(2)}, u32[]{:S(2)}) async-start(bf16[8,128,512]{2,1,0:T(8,128)(2,1)} %bitcast.72), calls=%async_computation | async-start | bytes 2097152 | tf_op jit(solution)/shard_map/all_to_all | solution.py:601
  11.0 10.3 %copy-start.10 = (s32[96,2]{0,1:T(2,128)S(1)}, s32[96,2]{0,1:T(2,128)}, u32[]{:S(2)}) copy-start(s32[96,2]{0,1:T(2,128)} %param.41) | copy-start | bytes 2308
  11.0 10.8 %copy-start.11 = (f32[128]{0:T(128)S(1)}, f32[128]{0:T(128)}, u32[]{:S(2)}) copy-start(f32[128]{0:T(128)} %param.38) | copy-start | bytes 1540
  11.0 10.9 %copy-start.6 = (f32[96,2]{0,1:T(2,128)S(1)}, f32[96,2]{0,1:T(2,128)}, u32[]{:S(2)}) copy-start(f32[96,2]{0,1:T(2,128)} %param.42) | copy-start | bytes 2308
  15.9 2.0 copy-start.1
  21.9 2.1 copy-start.7
  29.7 5.3 %copy-start.5 = (f32[8,128]{1,0:T(8,128)}, f32[8,128]{1,0:T(8,128)S(1)}, u32[]{:S(2)}) copy-start(f32[8,128]{1,0:T(8,128)S(1)} %scatter.9.route) | copy-start | bytes 12292
  95.5 4.2 %copy-start.12 = (bf16[32,2,48,512]{3,2,1,0:T(8,128)(2,1)S(1)}, bf16[32,2,48,512]{3,2,1,0:T(8,128)(2,1)}, u32[]{:S(2)}) copy-start(bf16[32,2,48,512]{3,2,1,0:T(8,128)(2,1)} %get-tuple-element.36) | copy-start | bytes 9437188
  95.5 4.2 %copy-start.13 = (bf16[512,192]{0,1:T(8,128)(2,1)S(1)}, bf16[512,192]{0,1:T(8,128)(2,1)}, u32[]{:S(2)}) copy-start(bf16[512,192]{0,1:T(8,128)(2,1)} %param.47) | copy-start | bytes 589828
  95.5 4.2 %copy-start.14 = (bf16[512,192]{0,1:T(8,128)(2,1)S(1)}, bf16[512,192]{0,1:T(8,128)(2,1)}, u32[]{:S(2)}) copy-start(bf16[512,192]{0,1:T(8,128)(2,1)} %param.46) | copy-start | bytes 589828
  182.2 3.0 %copy-start.2 = (bf16[8,2,192,192]{3,2,1,0:T(8,128)(2,1)S(1)}, bf16[8,2,192,192]{3,2,1,0:T(8,128)(2,1)}, u32[]{:S(2)}) copy-start(bf16[8,2,192,192]{3,2,1,0:T(8,128)(2,1)} %get-tuple-element.38) | copy-start | bytes 3538948
  182.2 3.0 %copy-start.4 = (bf16[192,512]{1,0:T(8,128)(2,1)S(1)}, bf16[192,512]{1,0:T(8,128)(2,1)}, u32[]{:S(2)}) copy-start(bf16[192,512]{1,0:T(8,128)(2,1)} %param.48) | copy-start | bytes 589828

commit v2 on v1

--- a/solution.py
+++ b/solution.py
@@ -13,6 +13,7 @@
 STATE = 64
 EP = ("ep_0", "ep_1")
 MESH = pl.DeviceIdType.MESH
+LAG_EP, LAG_TP, LAG_CORE, GAP = 4.0, 7.0, 3.0, 3.4
 
 
 class Node:
@@ -52,9 +53,9 @@
     return nodes
 
 
-def tp_tree(tp_count, chunks):
+def tp_tree(tp_count, chunks, only=None):
     nodes = []
-    for chunk in range(chunks):
+    for chunk in range(chunks) if only is None else only:
         root = Node(chunk, (0, 0), None, None)
         line = chain(chunk, root, 0, "y", tp_count // 2, chunk % 2 == 0)
         for node in line:
@@ -77,7 +78,8 @@
             price = cost * (0.35 if kid.move[0] == "core" else 1.0)
             start = max(now, free.get(kid.move, 0.0))
             free[kid.move] = start + price
-            kid.sent, kid.came = start, start + price + lag
+            kid.sent = start
+            kid.came = start + price + (LAG_CORE if kid.move[0] == "core" else lag)
             heapq.heappush(heap, (kid.came, place[id(kid)]))
     for i, node in enumerate(order):
         node.index = i
@@ -86,32 +88,44 @@
 
 class Places:
     def __init__(self, kind, sizes):
-        self.kind, self.sizes = kind, sizes
+        self.kind, self.sizes, self.known, self.flats = kind, sizes, {}, {}
         if kind == "ep":
             self.me = (lax.axis_index("ep_0"), lax.axis_index("ep_1"))
         else:
             t = lax.axis_index("tp")
             self.me = (t // 2, t % 2)
 
+    def along(self, axis, off):
+        size = self.sizes[axis]
+        off = off % size
+        if off == 0:
+            return self.me[axis]
+        if (axis, off) not in self.known:
+            self.known[axis, off] = lax.rem(self.me[axis] + off, size)
+        return self.known[axis, off]
+
     def shifted(self, off):
-        return tuple(
-            lax.rem(m + (o + s), s) for m, o, s in zip(self.me, off, self.sizes)
-        )
+        return tuple(self.along(axis, o) for axis, o in enumerate(off))
 
     def flat(self, at):
         return at[0] * self.sizes[1] + at[1]
 
-    def owner(self, off, sign=-1):
-        return self.flat(self.shifted(tuple(sign * o for o in off)))
+    def owner(self, off):
+        return self.at(tuple(-o for o in off))
+
+    def at(self, off):
+        key = tuple(o % size for o, size in zip(off, self.sizes))
+        if key not in self.flats:
+            self.flats[key] = self.flat(self.shifted(key))
+        return self.flats[key]
 
     def device(self, move, sign=1):
         name, step = move
         step = step * sign
         if self.kind == "ep":
             axis = EP.index(name)
-            return {name: lax.rem(self.me[axis] + (step + self.sizes[axis]), self.sizes[axis])}
-        off = (step, 0) if name == "y" else (0, step)
-        return {"tp": self.flat(self.shifted(off))}
+            return {name: self.along(axis, step)}
+        return {"tp": self.at((step, 0) if name == "y" else (0, step))}
 
     def greet(self):
         barrier = pltpu.get_barrier_semaphore()
@@ -160,16 +174,16 @@
     return started
 
 
-def add_into(out, terms, rows, step=16):
-    def body(i, _):
-        at = pl.ds(pl.multiple_of(i * step, step), step)
+def add_into(out, terms, rows, step=48):
+    def body(i):
+        at = pl.ds(i * step, step)
         total = terms[0](at).astype(jnp.float32)
         for term in terms[1:]:
             total = total + term(at).astype(jnp.float32)
         out(at, total)
-        return 0
-
-    lax.fori_loop(0, rows // step, body, 0)
+
+    for i in range(rows // step):
+        body(i)
 
 
 def reduce_events(order, places, view, load, put, slots, sums, rows, send, recv, events, base=0.0):
@@ -335,106 +349,229 @@
     )(reads, weights, tokens, gain, gate, route)
 
 
-def spread_kernel(order, small, sizes, block, extra, out, out_extra, send, recv, send2, recv2):
-    places = Places("ep", sizes)
-    places.greet()
-    mine = places.flat(places.me)
-    events = []
-    one = gather_events(
-        order, places, lambda c: block.at[c], lambda c, b: out.at[b, c], send, recv, events
-    )
-    two = gather_events(
-        small, places, lambda c: extra, lambda c, b: out_extra.at[b], send2, recv2, events, 0.1
-    )
-    out[mine] = block[...]
-    out_extra[mine] = extra[...]
-    run_events(events, (one, two))
-
-
-def spread(block, extra, sizes):
-    count = sizes[0] * sizes[1]
-    order = timed(ep_tree(sizes), 1.0, 1.8)
-    small = timed([n for n in ep_tree(sizes) if n.chunk == 0], 0.1, 1.8)
-    return pl.pallas_call(
-        functools.partial(spread_kernel, order, small, sizes),
-        out_shape=(
-            jax.ShapeDtypeStruct((count, *block.shape), block.dtype),
-            jax.ShapeDtypeStruct((count, *extra.shape), extra.dtype),
-        ),
-        in_specs=vmem(2),
-        out_specs=tuple(vmem(2)),
-        scratch_shapes=dma_sems(order) + dma_sems(small),
-        compiler_params=params(2),
-        name="spread",
-    )(block, extra)
-
-
-def expert_in_kernel(
-    order, order2, order3, sizes, half, rows, wide,
-    full, hid_all, mine, slots, sums, send, recv, send2, recv2, send3, recv3,
+def forward_plan(sizes, tp_count):
+    big = timed(ep_tree(sizes), 1.06, LAG_EP)
+    small = timed([n for n in ep_tree(sizes) if n.chunk == 0], 0.1, LAG_EP)
+    ready = {}
+    for node in big + small:
+        dz = node.off[0] % sizes[0]
+        ready[dz] = max(ready.get(dz, 0.0), node.came)
+    ranks, base = [], 0.0
+    for dz in sorted(ready, key=lambda d: ready[d]):
+        base = max(ready[dz] + 1.0, base + GAP)
+        ranks.append((dz, base))
+    flows = []
+    for rank, (dz, base) in enumerate(ranks):
+        trees = [timed(tp_tree(tp_count, 2, (rank % 2,)), cost, LAG_TP) for cost in (1.06, 0.8, 0.4)]
+        flows.append((dz, base, trees))
+    return big, small, flows
+
+
+def forward_kernel(
+    big, small, flows, sizes, tp_sizes, capacity,
+    block, extra, both, gate_hbm, up_hbm, down_hbm,
+    partial, hid_all, extra_all,
+    out, wide, rows, full, mine, slots, sums, gate_w, up_w, down_w, gate_val, hidden,
+    send, recv, send2, recv2, send3, recv3, send4, recv4, send5, recv5, loaded,
 ):
-    places = Places("tp", sizes)
-    places.greet()
-    me = places.flat(places.me)
-    part = rows.shape[2]
-    span = rows.shape[1]
-    events, f32 = [], jnp.float32
+    f32, bf16 = jnp.float32, jnp.bfloat16
+    loads = [
+        pltpu.make_async_copy(src, dst, loaded.at[i])
+        for i, (src, dst) in enumerate(((gate_hbm, gate_w), (up_hbm, up_w), (down_hbm, down_w)))
+    ]
+    for load in loads:
+        load.start()
+    places, tp = Places("ep", sizes), Places("tp", tp_sizes)
+    barrier = pltpu.get_barrier_semaphore()
+    for name in EP:
+        for step in (1, -1):
+            device = places.device((name, step))
+            pl.semaphore_signal(barrier, inc=1, device_id=device, device_id_type=MESH)
+    for move in (("y", 1), ("y", -1), ("core", 1)):
+        pl.semaphore_signal(barrier, inc=1, device_id=tp.device(move), device_id_type=MESH)
+    pl.semaphore_wait(barrier, 7)
+
+    mine_at = places.flat(places.me)
+    expert = mine_at.astype(f32)
+    me = tp.flat(tp.me)
+    zs, xs = sizes
+    _, half_rows, part = block.shape
+    seq = 2 * half_rows
+    span = capacity * xs
+    half = hidden.shape[1]
+    hid = both.shape[1] // 2
+    mine[...] = jnp.zeros_like(mine)
+    events, started = [], []
+    out[mine_at] = block[...]
+    extra_all[mine_at] = extra[...]
+    started.append(
+        gather_events(
+            big, places, lambda c: block.at[c], lambda c, b: out.at[b, c], send, recv, events
+        )
+    )
+    started.append(
+        gather_events(
+            small, places, lambda c: extra, lambda c, b: extra_all.at[b], send2, recv2, events, 0.1
+        )
+    )
+    lane = lax.broadcasted_iota(jnp.int32, (8, 128), 1)
+    before = lax.broadcasted_iota(jnp.int32, (128, 128), 0) < lax.broadcasted_iota(
+        jnp.int32, (128, 128), 1
+    )
+    before = before.astype(f32)
+    slot_at = lax.broadcasted_iota(jnp.int32, (span, 128), 0).astype(f32)
 
     def columns(b):
         return pl.ds(pl.multiple_of(b * part, part), part)
 
-    def put(chunk, at, value):
-        gate, up = value[:, :half], value[:, half:]
-        hidden = gate * jax.nn.sigmoid(gate) * up
-        mine[chunk, at, :] = hidden.astype(mine.dtype)
-
-    count = wide.shape[2]
-    one = reduce_events(
-        order2, places,
-        lambda c, b: wide.at[b, c], lambda c, b, at: wide[b, c, at, :], put,
-        slots, sums, count, send2, recv2, events,
-    )
-    lastly = max(at for at, _ in events)
-    two = gather_events(
-        order, places, lambda c: rows.at[c],
-        lambda c, b: full.at[pl.ds(c * span, span), columns(b)],
-        send, recv, events, 0.01,
-    )
-    three = gather_events(
-        order3, places, lambda c: mine.at[c], lambda c, b: hid_all.at[b, c],
-        send3, recv3, events, lastly + 0.01,
-    )
-    for c in range(rows.shape[0]):
-        full[pl.ds(c * span, span), columns(me)] = rows[c]
-    run_events(events, (one, two, three))
-    hid_all[me] = mine[...]
-
-
-def expert_in(rows, wide, half, tp_count):
-    sizes = (tp_count // 2, 2)
-    order = timed(tp_tree(tp_count, 2), 4.2, 1.0)
-    order2 = timed(tp_tree(tp_count, 2), 3.2, 1.0)
-    order3 = timed(tp_tree(tp_count, 2), 1.6, 1.0)
-    bf16 = rows.dtype
-    chunks, span, part = rows.shape
-    _, _, count, cols = wide.shape
+    def use_group(rank, dz):
+        first = pl.multiple_of(places.along(0, -dz) * xs, xs)
+        picked = jnp.zeros((span, part), f32)
+        for x in range(xs):
+            info = extra_all[first + x]
+            named = (info[1:2] == expert) | (info[2:3] == expert)
+            named = jnp.where(named & (lane[:1] < seq), 1.0, 0.0)
+            slot = jnp.dot(
+                jnp.broadcast_to(named, (8, 128)), before, preferred_element_type=f32
+            )[:1]
+            place = jnp.where(named > 0, slot + float(capacity * x), -1.0)
+            select = jnp.where(place == slot_at, 1.0, 0.0)[:, :seq].astype(bf16)
+            value = out[first + x].reshape(seq, part)
+            picked = picked + jnp.dot(select, value, preferred_element_type=f32)
+        rows[rank] = picked.astype(bf16)
+        full[pl.ds(rank * span, span), columns(me)] = picked.astype(bf16)
+        value = out[pl.ds(first, xs)].reshape(xs * seq, part)
+        product = jnp.dot(value, both[...], preferred_element_type=f32).astype(bf16)
+        wide[rank] = product.reshape(2 * xs, half_rows, product.shape[1])
+
+    nodes = len(flows[0][2][0])
+    row_time = []
+    for rank, (dz, base, (row_tree, sum_tree, hid_tree)) in enumerate(flows):
+        events.append((base - 0.1, functools.partial(use_group, rank, dz)))
+        sems = [
+            sem.at[pl.ds(rank * nodes, nodes)] for sem in (send3, recv3, send4, recv4, send5, recv5)
+        ]
+
+        def put(chunk, at, value, rank=rank):
+            gate, up = value[:, :hid], value[:, hid:]
+            mine[rank, at, :hid] = (gate * jax.nn.sigmoid(gate) * up).astype(bf16)
+
+        started.append(
+            reduce_events(
+                sum_tree, tp,
+                lambda c, b, r=rank: wide.at[r, b],
+                lambda c, b, at, r=rank: wide[r, b, at, :],
+                put, slots.at[rank], sums.at[rank], half_rows, sems[2], sems[3], events, base,
+            )
+        )
+        summed = base + max(node.came for node in sum_tree)
+        started.append(
+            gather_events(
+                row_tree, tp,
+                lambda c, r=rank: rows.at[r],
+                lambda c, b, r=rank: full.at[pl.ds(r * span, span), columns(b)],
+                sems[0], sems[1], events, base + 0.01,
+            )
+        )
+        row_time.append(base + 0.01 + max(node.came for node in row_tree))
+
+        def keep(rank, dz):
+            hid_all[places.along(0, -dz), me] = mine[rank]
+
+        events.append((summed + 0.01, functools.partial(keep, rank, dz)))
+
+        def hid_target(c, b, dz=dz):
+            return hid_all.at[places.along(0, -dz), b]
+
+        started.append(
+            gather_events(
+                hid_tree, tp, lambda c, r=rank: mine.at[r], hid_target,
+                sems[4], sems[5], events, summed + 0.02,
+            )
+        )
+
+    group_rows = full.shape[0] // 2
+
+    def gate_part(h):
+        if h == 0:
+            loads[0].wait()
+        value = full[pl.ds(h * group_rows, group_rows), :]
+        gate_val[...] = jnp.dot(value, gate_w[...], preferred_element_type=f32)
+
+    def up_part(h):
+        if h == 0:
+            loads[1].wait()
+        value = full[pl.ds(h * group_rows, group_rows), :]
+        up_val = jnp.dot(value, up_w[...], preferred_element_type=f32)
+        gate = gate_val[...]
+        hidden[...] = (gate * jax.nn.sigmoid(gate) * up_val).astype(bf16)
+
+    def down_part(h, piece, pieces):
+        if h == 0 and piece == 0:
+            loads[2].wait()
+        width = partial.shape[2] // pieces
+        at = slice(piece * width, (piece + 1) * width)
+        product = jnp.dot(hidden[...], down_w[:, at], preferred_element_type=f32)
+        partial[h, :, at] = product.astype(bf16)
+
+    for h in range(2):
+        when = max(row_time[h * len(flows) // 2 : (h + 1) * len(flows) // 2]) + 0.02
+        if h == 1:
+            when = max(when, max(at for at, _ in events) + 0.02)
+        step = 1.5
+        events.append((when, functools.partial(gate_part, h)))
+        events.append((when + step, functools.partial(up_part, h)))
+        for piece in range(4):
+            act = functools.partial(down_part, h, piece, 4)
+            events.append((when + step * 2 + piece * step / 2, act))
+    run_events(events, started)
+
+
+def forward(block, extra, both, gate_w, up_w, down_w, sizes, tp_count, capacity):
+    count = sizes[0] * sizes[1]
+    tp_sizes = (tp_count // 2, 2)
+    big, small, flows = forward_plan(sizes, tp_count)
+    bf16, f32 = block.dtype, jnp.float32
+    _, half_rows, part = block.shape
+    span = capacity * sizes[1]
+    slots = capacity * count
+    width = part * tp_count
+    half = gate_w.shape[1]
+    hid = both.shape[1] // 2
+    lanes = -(-hid // 128) * 128
+    groups = sizes[0]
+    nodes = groups * len(flows[0][2][0])
+    anywhere = [pl.BlockSpec(memory_space=pl.ANY)] * 3
     return pl.pallas_call(
-        functools.partial(expert_in_kernel, order, order2, order3, sizes, half),
+        functools.partial(forward_kernel, big, small, flows, sizes, tp_sizes, capacity),
         out_shape=(
-            jax.ShapeDtypeStruct((chunks * span, part * tp_count), bf16),
-            jax.ShapeDtypeStruct((tp_count, 2, count, half), bf16),
+            jax.ShapeDtypeStruct((2, slots // 2, width), bf16),
+            jax.ShapeDtypeStruct((groups, tp_count, half_rows, lanes), bf16),
+            jax.ShapeDtypeStruct((count, *extra.shape), f32),
         ),
-        in_specs=vmem(2),
-        out_specs=tuple(vmem(2)),
+        in_specs=vmem(3) + anywhere,
+        out_specs=tuple(vmem(3)),
         scratch_shapes=[
-            pltpu.VMEM((2, count, half), bf16),
-            pltpu.VMEM((len(order2), count, cols), bf16),
-            pltpu.VMEM((len(order2), count, cols), bf16),
+            pltpu.VMEM((count, 2, half_rows, part), bf16),
+            pltpu.VMEM((groups, tp_count, half_rows, 2 * hid), bf16),
+            pltpu.VMEM((groups, span, part), bf16),
+            pltpu.VMEM((slots, width), bf16),
+            pltpu.VMEM((groups, half_rows, lanes), bf16),
+            pltpu.VMEM((groups, nodes // groups, half_rows, 2 * hid), bf16),
+            pltpu.VMEM((groups, nodes // groups, half_rows, 2 * hid), bf16),
+            pltpu.VMEM(gate_w.shape, bf16),
+            pltpu.VMEM(up_w.shape, bf16),
+            pltpu.VMEM(down_w.shape, bf16),
+            pltpu.VMEM((slots // 2, half), f32),
+            pltpu.VMEM((slots // 2, half), bf16),
         ]
-        + dma_sems(order) + dma_sems(order2) + dma_sems(order3),
-        compiler_params=params(3),
-        name="expert_in",
-    )(rows, wide)
+        + dma_sems(big)
+        + dma_sems(small)
+        + [pltpu.SemaphoreType.DMA((nodes,))] * 6
+        + [pltpu.SemaphoreType.DMA((3,))],
+        compiler_params=params(2),
+        name="forward",
+    )(block, extra, both, gate_w, up_w, down_w)
 
 
 def expert_out_kernel(order, sizes, partial, weight, out, slots, sums, send, recv):
@@ -461,7 +598,7 @@
 
 def expert_out(partial, weight, tp_count):
     sizes = (tp_count // 2, 2)
-    order = timed(tp_tree(tp_count, 2), 4.2, 1.0)
+    order = timed(tp_tree(tp_count, 2), 4.2, LAG_TP)
     chunks, span, width = partial.shape
     part = width // tp_count
     bf16 = partial.dtype
@@ -492,7 +629,7 @@
 
 
 def collect(blocks, resid, sizes):
-    order = timed(ep_tree(sizes), 1.0, 1.8)
+    order = timed(ep_tree(sizes), 1.06, LAG_EP)
     _, _, rows, cols = blocks.shape
     bf16 = blocks.dtype
     return pl.pallas_call(
@@ -614,8 +751,14 @@
         tp_count, width
     )
     sizes = (lax.axis_size("ep_0"), lax.axis_size("ep_1"))
-    everyone, branch_all = spread(normed_two, branch, sizes)
-    everyone = everyone.reshape(ep_count * seq_count, part_width)
+    both_proj = jnp.concatenate([dense_gate, dense_up], axis=1)
+    partial, dense_hidden, branch_all = forward(
+        normed_two, branch, both_proj, expert_gate[0], expert_up[0], expert_down[0],
+        sizes, tp_count, capacity,
+    )
+    dense_hidden = dense_hidden.reshape(ep_count * seq_count, -1)
+    spare = dense_hidden.shape[1] - dense_down.shape[0]
+    dense_down = jnp.pad(dense_down, ((0, spare), (0, 0)))
     route_all = branch_all[:, 1:, :seq_count]
     match = (route_all[:, :top_count] == ep_index.astype(f32)).astype(f32)
     named = jnp.sum(match, axis=1)
@@ -623,30 +766,21 @@
     order = jnp.arange(seq_count)
     before = (order[:, None] < order[None, :]).astype(f32)
     slot = jnp.dot(named, before, preferred_element_type=f32)
-    place = slot + capacity * jnp.arange(ep_count, dtype=f32)[:, None]
+    group = jnp.arange(ep_count, dtype=jnp.int32) // sizes[1]
+    offset = lax.rem(lax.axis_index("ep_0") - group + sizes[0], sizes[0])
+    rank = jnp.zeros((ep_count,), f32)
+    for at, (dz, _, _) in enumerate(forward_plan(sizes, tp_count)[2]):
+        rank = jnp.where(offset == dz % sizes[0], float(at), rank)
+    within = (jnp.arange(ep_count, dtype=jnp.int32) % sizes[1]).astype(f32)
+    place = slot + capacity * (rank * sizes[1] + within)[:, None]
     place = jnp.where(named > 0, place, -1.0).reshape(-1)
     select = place[None, :] == jnp.arange(slots, dtype=f32)[:, None]
     select = select.astype(bf16)
     row_weight = jnp.sum(select.astype(f32) * weight_all[None, :], axis=1)
     branch_all = branch_all[:, 0, :seq_count].reshape(ep_count * seq_count, 1)
 
-    both_proj = jnp.concatenate([dense_gate, dense_up], axis=1)
-    hidden_width = dense_gate.shape[1]
-    wide = jnp.dot(everyone, both_proj, preferred_element_type=f32).astype(bf16)
-    rows_in = jnp.dot(select, everyone, preferred_element_type=f32).astype(bf16)
-    full_rows, dense_hidden = expert_in(
-        rows_in.reshape(2, slots // 2, part_width),
-        wide.reshape(tp_count, 2, -1, 2 * hidden_width),
-        hidden_width,
-        tp_count,
-    )
-    dense_hidden = dense_hidden.reshape(ep_count * seq_count, hidden_width)
-    gate_val = jnp.dot(full_rows, expert_gate[0], preferred_element_type=f32)
-    up_val = jnp.dot(full_rows, expert_up[0], preferred_element_type=f32)
-    hidden = (jax.nn.silu(gate_val) * up_val).astype(bf16)
-    partial = jnp.dot(hidden, expert_down[0], preferred_element_type=f32).astype(bf16)
     row_weight = jnp.broadcast_to(row_weight[:, None], (slots, 128)).reshape(2, slots // 2, 128)
-    weighted = expert_out(partial.reshape(2, slots // 2, width), row_weight, tp_count)
+    weighted = expert_out(partial, row_weight, tp_count)
     weighted = weighted.reshape(slots, part_width)
 
     dense_part = jnp.dot(dense_hidden, dense_down, preferred_element_type=f32)

time: 225 us -> 177 us (0.79)
  matrix products: 34.1 us -> 8.74 us
  Pallas kernels: 156 us -> 140 us
  local copies, waits for them, and re-layouts: 17.5 us -> 14.5 us
    dot_general x4 -> x0, matrix products: 21 us -> none  [the longest x1 8.06 us: shards(): jnp.dot(hidden, expert_down[0], preferred_element_type=f32).astype(bf16)]
    pallas_call x2 -> x1, Pallas kernels: 86.3 us -> 71.4 us  [forward(): pl.pallas_call(functools.partial(forward_kernel, big, small, flows, sizes...]
    unnamed x35 -> x33, local copies, waits for them, and re-layouts: 1.62 us -> 4.7 us
    pallas_call x1, Pallas kernels: 34.2 us -> 31.2 us  [collect(): pl.pallas_call(functools.partial(collect_kernel, order, sizes), out_shape...]
    slice x2, local copies, waits for them, and re-layouts: 2.85 us -> 0.15 us  [state_step(): old_re = states[0].reshape(count, groups, STATE)]
    another operation x2, local copies, waits for them, and re-layouts: 2.56 us -> 0.25 us  [state_step(): jnp.stack([new_re.reshape(count, groups * STATE), new_im.reshape(count, g...]
  transfers between devices with their start and end apart: 1 -> 1, of which waited for: 0 -> 0; matrix products, arithmetic and copies ran while one was open for 11% -> 9% of each run, Pallas kernels for 0% -> 0%
where the time goes in v2:
time: 177 us; the launch traced here: 176 us
  Pallas kernels  140 us (79%)
  local copies, waits for them, and re-layouts  14.5 us (8%)
  matrix products  8.74 us (5%)
  other arithmetic  6.68 us (4%)
  starting transfers between devices  5.77 us (3%)
    pallas_call x1, Pallas kernels, forward(): pl.pallas_call(functools.partial(forward_kernel, big, small, flows, sizes...  71.4 us
    pallas_call x1, Pallas kernels, collect(): pl.pallas_call(functools.partial(collect_kernel, order, sizes), out_shape...  31.2 us
    pallas_call x1, Pallas kernels, expert_out(): pl.pallas_call(functools.partial(expert_out_kernel, order, sizes), out_sh...  24 us
    pallas_call x1, Pallas kernels, mix(): pl.pallas_call(functools.partial(mix_kernel, tp_count, width), out_shape=...  13 us
    all_to_all x1, starting transfers between devices, shards(): lax.all_to_all(split_up(out_proj, 1, tp_count), 'tp', 0, 0, tiled=True)  5.77 us
    unnamed x33, local copies, waits for them, and re-layouts  4.7 us
  transfers between devices with their start and end apart: 1, of which 0 were waited for; matrix products, arithmetic and copies ran while one was open for 9% of the time, Pallas kernels for 0%

profile of v2, /device:TPU:8, one launch (start us, length us, event | category | flops | bytes accessed | tf_op | source)
XLA Modules:
  0.0 176.3 jit_solution(14703316554324677314)
XLA Ops:
  0.6 0.0 copy-start
  0.7 0.0 copy-start.3
  0.7 2.4 %copy.64 = bf16[16,8,8,512]{3,2,0,1:T(8,128)(2,1)} copy(bf16[16,8,8,512]{3,2,1,0:T(8,128)(2,1)} %bitcast.63) | data formatting | bytes 2097152 | tf_op jit(solution)/shard_map/reshape | solution.py:648
  3.1 5.8 %all-to-all-start = ((bf16[8,128,512]{2,1,0:T(8,128)(2,1)}), bf16[8,128,512]{2,1,0:T(8,128)(2,1)S(1)}, u32[]{:S(2)}, u32[]{:S(2)}) async-start(bf16[8,128,512]{2,1,0:T(8,128)(2,1)} %bitcast.49), calls=%async_computation | async-start | bytes 2097152 | tf_op jit(solution)/shard_map/all_to_all | solution.py:738
  8.9 0.5 exp.9
  9.4 0.3 fusion.3
  9.7 0.0 copy-start.12
  9.7 0.4 convolution_convert_fusion
  10.2 0.1 copy.51
  10.3 0.1 copy.49
  10.5 0.1 copy.50
  10.6 0.8 add_divide_fusion
  11.4 0.3 fusion.6
  11.7 0.3 fusion.7
  12.1 0.7 mul.226
  12.8 1.0 fusion.43
  13.8 1.0 fusion.9
  14.8 1.1 copy.58
  15.9 1.1 copy.59
  17.0 0.1 copy.56
  17.0 0.1 copy.61
  17.2 0.1 copy.60
  17.3 1.3 dynamic_slice.10
  18.6 0.5 scatter.9.route
  19.2 1.3 dynamic-slice_convert_fusion
  20.5 1.5 constant_dynamic-slice_fusion.tokens
  22.0 0.9 pad_maximum_fusion.both
  22.9 0.8 pad_maximum_fusion.1
  23.7 0.6 fusion.28.reads
  24.3 0.0 all-to-all-done
  24.3 1.0 copy-done.1
  25.3 13.0 %mix.1 = (bf16[2,48,512]{2,1,0:T(8,128)(2,1)}, bf16[96,512]{1,0:T(8,128)(2,1)}, f32[8,128]{1,0:T(8,128)}) custom-call(bf16[96,128]{1,0:T(8,128)(2,1)} %fusion.28.reads, bf16[1024,512]{1,0:T(8,128)(2,1)} %bitcast.51, bf16[96,512]{1,0:T(8,128)(2,1)} %constant_dynamic-slice_fusion.tokens, f32[1,512]{1,0:T(1,128)} %bitcast.71, f32[1,512]{1,0:T(1,128)} %bitcast.70, ...), custom_call_target="tpu_custom_call" | custom-call | tf_op jit(solution)/shard_map/mix/pallas_call | solution.py:333
  38.3 71.4 %forward.1 = (bf16[2,192,4096]{2,1,0:T(8,128)(2,1)}, bf16[8,8,48,256]{3,2,1,0:T(8,128)(2,1)}, f32[32,8,128]{2,1,0:T(8,128)}) custom-call(bf16[2,48,512]{2,1,0:T(8,128)(2,1)} %get-tuple-element.32.block, f32[8,128]{1,0:T(8,128)} %get-tuple-element.33.extra, bf16[512,384]{1,0:T(8,128)(2,1)} %pad_maximum_fusion.both, bf16[4096,384]{1,0:T(8,128)(2,1)} %bitcast.52, ...), custom_call_target="tpu_custom_call" | custom-call | tf_op jit(solution)/shard_map/forward/pallas_call | solution.py:545
  109.7 0.9 slice_reduce_fusion
  110.7 1.1 convert_reduce_fusion
  111.8 0.1 mul.245
  111.9 0.1 fusion.10
  112.0 0.1 eq.96
  112.0 0.1 mul.242
  112.1 0.8 multiply_reduce_fusion
  112.9 0.1 broadcast_in_dim.76
  113.0 0.8 broadcast_in_dim.77.weight
  113.8 24.0 %expert_out.1 = bf16[2,192,512]{2,1,0:T(8,128)(2,1)} custom-call(bf16[2,192,4096]{2,1,0:T(8,128)(2,1)} %get-tuple-element.35.partial, f32[2,192,128]{2,1,0:T(8,128)} %broadcast_in_dim.77.weight), custom_call_target="tpu_custom_call" | custom-call | tf_op jit(solution)/shard_map/expert_out/pallas_call | solution.py:605
  137.8 0.0 copy-start.7
  137.9 3.0 %fusion = f32[3072,512]{1,0:T(8,128)S(1)} fusion(bf16[384,512]{1,0:T(8,128)(2,1)} %bitcast.62, f32[3072]{0:T(1024)S(1)} %eq.96), kind=kOutput, calls=%fused_computation.3 | convolution fusion | flops 1209139200 | bytes 6696960 | tf_op jit(solution)/shard_map/dot_general | solution.py:787
  140.9 2.7 %add_convert_fusion = bf16[3072,512]{1,0:T(8,128)(2,1)} fusion(f32[3072,512]{1,0:T(8,128)S(1)} %fusion, bf16[3072,256]{1,0:T(8,128)(2,1)S(1)} %bitcast.61, f32[3072]{0:T(1024)S(1)} %mul.245, bf16[192,512]{1,0:T(8,128)(2,1)S(1)} %copy-done.7), kind=kOutput, calls=%fused_computation | convolution fusion | flops 810024960 | bytes 11218944 | tf_op jit(solution)/shard_map/dot_general | solution.py:786
  143.5 31.2 %collect.1 = bf16[2,48,512]{2,1,0:T(8,128)(2,1)} custom-call(bf16[32,2,48,512]{3,2,1,0:T(8,128)(2,1)} %bitcast.50, bf16[2,48,512]{2,1,0:T(8,128)(2,1)} %bitcast.69), custom_call_target="tpu_custom_call" | custom-call | tf_op jit(solution)/shard_map/collect/pallas_call | solution.py:635
  174.8 1.5 copy.67
  (33 shorter events, 0.2 us)
Async XLA Ops:
  0.6 9.1 %copy-start = (bf16[4096,128]{1,0:T(8,128)(2,1)S(1)}, bf16[4096,128]{1,0:T(8,128)(2,1)}, u32[]{:S(2)}) copy-start(bf16[4096,128]{1,0:T(8,128)(2,1)} %param.30) | copy-start | bytes 3145732
  0.6 8.3 %copy-start.14 = (f32[8]{0:T(128)S(1)}, f32[8]{0:T(128)}, u32[]{:S(2)}) copy-start(f32[8]{0:T(128)} %param.33) | copy-start | bytes 100
  0.7 8.8 %copy-start.3 = (bf16[96,4096]{1,0:T(8,128)(2,1)S(1)}, bf16[96,4096]{1,0:T(8,128)(2,1)}, u32[]{:S(2)}) copy-start(bf16[96,4096]{1,0:T(8,128)(2,1)} %param.27) | copy-start | bytes 2359300
  0.7 9.1 %copy-start.13 = (f32[4096]{0:T(1024)S(1)}, f32[4096]{0:T(1024)}, u32[]{:S(2)}) copy-start(f32[4096]{0:T(1024)} %param.28) | copy-start | bytes 49156
  0.7 9.6 %copy-start.4 = (f32[2,96,512]{2,1,0:T(8,128)S(1)}, f32[2,96,512]{2,1,0:T(8,128)}, u32[]{:S(2)}) copy-start(f32[2,96,512]{2,1,0:T(8,128)} %param.39) | copy-start | bytes 1179652
  3.1 7.5 %copy-start.10 = (f32[8,64]{1,0:T(8,128)S(1)}, f32[8,64]{1,0:T(8,128)}, u32[]{:S(2)}) copy-start(f32[8,64]{1,0:T(8,128)} %param.32) | copy-start | bytes 6148
  3.1 7.5 %copy-start.11 = (f32[8,64]{1,0:T(8,128)S(1)}, f32[8,64]{1,0:T(8,128)}, u32[]{:S(2)}) copy-start(f32[8,64]{1,0:T(8,128)} %param.31) | copy-start | bytes 6148
  3.1 8.3 %copy-start.5 = (f32[8,64,16]{1,2,0:T(8,128)S(1)}, f32[8,64,16]{1,2,0:T(8,128)}, u32[]{:S(2)}) copy-start(f32[8,64,16]{1,2,0:T(8,128)} %param.35) | copy-start | bytes 98308
  3.1 8.3 %copy-start.6 = (f32[8,64,16]{1,2,0:T(8,128)S(1)}, f32[8,64,16]{1,2,0:T(8,128)}, u32[]{:S(2)}) copy-start(f32[8,64,16]{1,2,0:T(8,128)} %param.34) | copy-start | bytes 98308
  3.1 21.2 %all-to-all-start = ((bf16[8,128,512]{2,1,0:T(8,128)(2,1)}), bf16[8,128,512]{2,1,0:T(8,128)(2,1)S(1)}, u32[]{:S(2)}, u32[]{:S(2)}) async-start(bf16[8,128,512]{2,1,0:T(8,128)(2,1)} %bitcast.49), calls=%async_computation | async-start | bytes 2097152 | tf_op jit(solution)/shard_map/all_to_all | solution.py:738
  9.7 2.3 %copy-start.9 = (f32[96,2]{0,1:T(2,128)S(1)}, f32[96,2]{0,1:T(2,128)}, u32[]{:S(2)}) copy-start(f32[96,2]{0,1:T(2,128)} %param.42) | copy-start | bytes 2308
  9.7 5.1 %copy-start.12 = (s32[96,2]{0,1:T(2,128)S(1)}, s32[96,2]{0,1:T(2,128)}, u32[]{:S(2)}) copy-start(s32[96,2]{0,1:T(2,128)} %param.41) | copy-start | bytes 2308
  19.1 5.2 %copy-start.8 = (f32[8,128]{1,0:T(8,128)}, f32[8,128]{1,0:T(8,128)S(1)}, u32[]{:S(2)}) copy-start(f32[8,128]{1,0:T(8,128)S(1)} %scatter.9.route) | copy-start | bytes 12292
  24.3 1.0 copy-start.1
  137.8 3.0 %copy-start.2 = (bf16[8,8,48,256]{3,2,1,0:T(8,128)(2,1)S(1)}, bf16[8,8,48,256]{3,2,1,0:T(8,128)(2,1)}, u32[]{:S(2)}) copy-start(bf16[8,8,48,256]{3,2,1,0:T(8,128)(2,1)} %get-tuple-element.36) | copy-start | bytes 4718596
  137.8 3.0 %copy-start.7 = (bf16[192,512]{1,0:T(8,128)(2,1)S(1)}, bf16[192,512]{1,0:T(8,128)(2,1)}, u32[]{:S(2)}) copy-start(bf16[192,512]{1,0:T(8,128)(2,1)} %param.48) | copy-start | bytes 589828

commit v3 on v2

--- a/solution.py
+++ b/solution.py
@@ -13,7 +13,7 @@
 STATE = 64
 EP = ("ep_0", "ep_1")
 MESH = pl.DeviceIdType.MESH
-LAG_EP, LAG_TP, LAG_CORE, GAP = 4.0, 7.0, 3.0, 3.4
+LAG_EP, LAG_TP, LAG_CORE, LAG_BACK, GAP = 4.0, 7.0, 3.0, 4.0, 3.4
 
 
 class Node:
@@ -294,16 +294,17 @@
     for k, copy in enumerate(copies):
         copy.wait()
         total = total + part(held[k + 1], k + 1)
-    flt = tokens[...].astype(f32) + total.astype(jnp.bfloat16).astype(f32)
+    cols = pl.ds(pl.multiple_of(me * resid.shape[1], resid.shape[1]), resid.shape[1])
+    flt = tokens[:, cols].astype(f32) + total.astype(jnp.bfloat16).astype(f32)
     flt = flt.astype(jnp.bfloat16).astype(f32)
     resid[...] = flt.astype(jnp.bfloat16)
-    gained = flt * gain[...]
+    gained = flt * gain[:, cols]
     ones = jnp.ones((8, flt.shape[1]), f32)
     high = lax.Precision.HIGHEST
     turned = (((1,), (1,)), ((), ()))
     square = lax.dot_general(ones, flt * flt, turned, precision=high, preferred_element_type=f32)
     logit = lax.dot_general(
-        ones, gained * gate[...], turned, precision=high, preferred_element_type=f32
+        ones, gained * gate[:, cols].astype(f32), turned, precision=high, preferred_element_type=f32
     )
     rows = flt.shape[0]
     stats[0, 0, :, :rows] = square
@@ -328,7 +329,7 @@
 
 
 def mix(reads, weights, tokens, gain, gate, route, tp_count, width):
-    rows, cols = tokens.shape
+    rows, cols = tokens.shape[0], tokens.shape[1] // tp_count
     bf16, f32 = jnp.bfloat16, jnp.float32
     return pl.pallas_call(
         functools.partial(mix_kernel, tp_count, width),
@@ -349,6 +350,34 @@
     )(reads, weights, tokens, gain, gate, route)
 
 
+def greet_all(places, tp):
+    barrier = pltpu.get_barrier_semaphore()
+    for name in EP:
+        for step in (1, -1):
+            device = places.device((name, step))
+            pl.semaphore_signal(barrier, inc=1, device_id=device, device_id_type=MESH)
+    for move in (("y", 1), ("y", -1), ("core", 1)):
+        pl.semaphore_signal(barrier, inc=1, device_id=tp.device(move), device_id_type=MESH)
+    pl.semaphore_wait(barrier, 7)
+
+
+def chosen(info, expert, seq, span, offset):
+    lane = lax.broadcasted_iota(jnp.int32, (1, 128), 1)
+    before = lax.broadcasted_iota(jnp.int32, (128, 128), 0) < lax.broadcasted_iota(
+        jnp.int32, (128, 128), 1
+    )
+    slot_at = lax.broadcasted_iota(jnp.int32, (span, 128), 0).astype(jnp.float32)
+    named = (info[1:2] == expert) | (info[2:3] == expert)
+    named = jnp.where(named & (lane < seq), 1.0, 0.0)
+    slot = jnp.dot(
+        jnp.broadcast_to(named, (8, 128)),
+        before.astype(jnp.float32),
+        preferred_element_type=jnp.float32,
+    )[:1]
+    place = jnp.where(named > 0, slot + float(offset), -1.0)
+    return jnp.where(place == slot_at, 1.0, 0.0)
+
+
 def forward_plan(sizes, tp_count):
     big = timed(ep_tree(sizes), 1.06, LAG_EP)
     small = timed([n for n in ep_tree(sizes) if n.chunk == 0], 0.1, LAG_EP)
@@ -382,15 +411,7 @@
     for load in loads:
         load.start()
     places, tp = Places("ep", sizes), Places("tp", tp_sizes)
-    barrier = pltpu.get_barrier_semaphore()
-    for name in EP:
-        for step in (1, -1):
-            device = places.device((name, step))
-            pl.semaphore_signal(barrier, inc=1, device_id=device, device_id_type=MESH)
-    for move in (("y", 1), ("y", -1), ("core", 1)):
-        pl.semaphore_signal(barrier, inc=1, device_id=tp.device(move), device_id_type=MESH)
-    pl.semaphore_wait(barrier, 7)
-
+    greet_all(places, tp)
     mine_at = places.flat(places.me)
     expert = mine_at.astype(f32)
     me = tp.flat(tp.me)
@@ -414,13 +435,6 @@
             small, places, lambda c: extra, lambda c, b: extra_all.at[b], send2, recv2, events, 0.1
         )
     )
-    lane = lax.broadcasted_iota(jnp.int32, (8, 128), 1)
-    before = lax.broadcasted_iota(jnp.int32, (128, 128), 0) < lax.broadcasted_iota(
-        jnp.int32, (128, 128), 1
-    )
-    before = before.astype(f32)
-    slot_at = lax.broadcasted_iota(jnp.int32, (span, 128), 0).astype(f32)
-
     def columns(b):
         return pl.ds(pl.multiple_of(b * part, part), part)
 
@@ -429,13 +443,7 @@
         picked = jnp.zeros((span, part), f32)
         for x in range(xs):
             info = extra_all[first + x]
-            named = (info[1:2] == expert) | (info[2:3] == expert)
-            named = jnp.where(named & (lane[:1] < seq), 1.0, 0.0)
-            slot = jnp.dot(
-                jnp.broadcast_to(named, (8, 128)), before, preferred_element_type=f32
-            )[:1]
-            place = jnp.where(named > 0, slot + float(capacity * x), -1.0)
-            select = jnp.where(place == slot_at, 1.0, 0.0)[:, :seq].astype(bf16)
+            select = chosen(info, expert, seq, span, capacity * x)[:, :seq].astype(bf16)
             value = out[first + x].reshape(seq, part)
             picked = picked + jnp.dot(select, value, preferred_element_type=f32)
         rows[rank] = picked.astype(bf16)
@@ -574,73 +582,139 @@
     )(block, extra, both, gate_w, up_w, down_w)
 
 
-def expert_out_kernel(order, sizes, partial, weight, out, slots, sums, send, recv):
-    places = Places("tp", sizes)
-    places.greet()
-    chunks, span, part = out.shape
-    events = []
+def backward_plan(sizes, tp_count):
+    big = timed(ep_tree(sizes), 1.06, LAG_EP)
+    last = max(node.came for node in big)
+    ready = {}
+    for node in big:
+        dz = node.off[0] % sizes[0]
+        ready[dz] = max(ready.get(dz, 0.0), node.came)
+    flows, base, start = [], 0.0, 0.0
+    for rank, dz in enumerate(sorted(ready, key=lambda d: -ready[d])):
+        tree = timed(tp_tree(tp_count, 2, (rank % 2,)), 1.06, LAG_BACK)
+        done = base + max(node.came for node in tree) + 0.5
+        start = max(start, done - (last - ready[dz]))
+        flows.append((dz, base, done, tree))
+        base += 1.8
+    return big, flows, start + 0.1
+
+
+def backward_kernel(
+    big, flows, start, spots, sizes, tp_sizes, capacity,
+    partial, extra_all, hid_all, down, resid, output,
+    slots, sums, answer, dense, mine, slots2, sums2, send, recv, send2, recv2,
+):
+    f32, bf16 = jnp.float32, jnp.bfloat16
+    places, tp = Places("ep", sizes), Places("tp", tp_sizes)
+    greet_all(places, tp)
+    expert = places.flat(places.me).astype(f32)
+    zs, xs = sizes
+    _, half_rows, part = resid.shape
+    seq = 2 * half_rows
+    span = capacity * xs
+    events, started = [], []
+    nodes = len(flows[0][3])
+    per_half = partial.shape[1] // span
 
     def columns(b):
         return pl.ds(pl.multiple_of(b * part, part), part)
 
-    def load(c, b, at):
-        return partial[c, at, columns(b)]
-
-    def put(c, at, value):
-        out[c, at, :] = (value * weight[c, at, :1]).astype(out.dtype)
-
-    one = reduce_events(
-        order, places, lambda c, b: partial.at[c, :, columns(b)], load, put,
-        slots, sums, span, send, recv, events,
-    )
-    run_events(events, (one,))
-
-
-def expert_out(partial, weight, tp_count):
-    sizes = (tp_count // 2, 2)
-    order = timed(tp_tree(tp_count, 2), 4.2, LAG_TP)
-    chunks, span, width = partial.shape
-    part = width // tp_count
-    bf16 = partial.dtype
+    own = (
+        lax.broadcasted_iota(jnp.int32, (seq, 128), 0)
+        == lax.broadcasted_iota(jnp.int32, (seq, 128), 1)
+    ).astype(f32)
+
+    def dense_group(rank, dz):
+        group = places.along(0, -dz)
+        first = group * xs
+        value = hid_all[group].reshape(xs * seq, hid_all.shape[3])
+        product = jnp.dot(value, down[...], preferred_element_type=f32)
+        for x in range(xs):
+            branch = jnp.sum(own * extra_all[first + x][:1], axis=1, keepdims=True)
+            dense[rank, x] = product[x * seq : (x + 1) * seq] * branch
+
+    def combine(rank, dz):
+        first = places.along(0, -dz) * xs
+        picks, weight = [], jnp.zeros((span, 1), f32)
+        for x in range(xs):
+            info = extra_all[first + x]
+            select = chosen(info, expert, seq, span, capacity * x)
+            named = jnp.where(info[1:2] == expert, info[3:4], 0.0)
+            named = named + jnp.where(info[2:3] == expert, info[4:5], 0.0)
+            weight = weight + jnp.sum(select * named, axis=1, keepdims=True)
+            picks.append(select[:, :seq].astype(bf16))
+        value = (answer[rank] * weight).astype(bf16)
+        for x in range(xs):
+            routed = lax.dot_general(
+                picks[x], value, (((0,), (0,)), ((), ())), preferred_element_type=f32
+            )
+            total = (routed + dense[rank, x]).astype(bf16)
+            mine[first + x] = total.reshape(2, half_rows, part)
+
+    for rank, (dz, base, done, tree) in enumerate(flows):
+        spot = spots[dz]
+        half, at_row = spot // per_half, (spot % per_half) * span
+
+        def put(chunk, at, value, rank=rank):
+            answer[rank, at, :] = value.astype(bf16).astype(f32)
+
+        started.append(
+            reduce_events(
+                tree, tp,
+                lambda c, b, h=half, r=at_row: partial.at[h, pl.ds(r, span), columns(b)],
+                lambda c, b, at, h=half, r=at_row: partial[
+                    h, pl.ds(r + at.start, at.size), columns(b)
+                ],
+                put, slots.at[rank], sums.at[rank], span,
+                send.at[pl.ds(rank * nodes, nodes)], recv.at[pl.ds(rank * nodes, nodes)],
+                events, base,
+            )
+        )
+        events.append((base + 1.0, functools.partial(dense_group, rank, dz)))
+        events.append((done, functools.partial(combine, rank, dz)))
+
+    def finish(c, at, value):
+        output[c, at, :] = (resid[c, at, :].astype(f32) + value).astype(output.dtype)
+
+    started.append(
+        reduce_events(
+            big, places, lambda c, b: mine.at[b, c], lambda c, b, at: mine[b, c, at, :], finish,
+            slots2, sums2, half_rows, send2, recv2, events, start,
+        )
+    )
+    run_events(events, started)
+
+
+def backward(partial, extra_all, hid_all, down, resid, sizes, tp_count, capacity):
+    big, flows, start = backward_plan(sizes, tp_count)
+    order = [dz for dz, _, _ in forward_plan(sizes, tp_count)[2]]
+    spots = {dz: at for at, dz in enumerate(order)}
+    bf16, f32 = partial.dtype, jnp.float32
+    _, half_rows, part = resid.shape
+    span = capacity * sizes[1]
+    groups, nodes = sizes[0], len(flows[0][3])
+    count = sizes[0] * sizes[1]
     return pl.pallas_call(
-        functools.partial(expert_out_kernel, order, sizes),
-        out_shape=jax.ShapeDtypeStruct((chunks, span, part), bf16),
-        in_specs=vmem(2),
+        functools.partial(
+            backward_kernel, big, flows, start, spots, sizes, (tp_count // 2, 2), capacity
+        ),
+        out_shape=jax.ShapeDtypeStruct(resid.shape, bf16),
+        in_specs=vmem(5),
         out_specs=vmem(1)[0],
-        scratch_shapes=[pltpu.VMEM((len(order), span, part), bf16)] * 2 + dma_sems(order),
+        scratch_shapes=[
+            pltpu.VMEM((groups, nodes, span, part), bf16),
+            pltpu.VMEM((groups, nodes, span, part), bf16),
+            pltpu.VMEM((groups, span, part), f32),
+            pltpu.VMEM((groups, sizes[1], 2 * half_rows, part), f32),
+            pltpu.VMEM((count, 2, half_rows, part), bf16),
+            pltpu.VMEM((len(big), half_rows, part), bf16),
+            pltpu.VMEM((len(big), half_rows, part), bf16),
+        ]
+        + [pltpu.SemaphoreType.DMA((groups * nodes,))] * 2
+        + dma_sems(big),
         compiler_params=params(4),
-        name="expert_out",
-    )(partial, weight)
-
-
-def collect_kernel(order, sizes, blocks, resid, out, slots, sums, send, recv):
-    places = Places("ep", sizes)
-    places.greet()
-    events = []
-
-    def put(c, at, value):
-        out[c, at, :] = (resid[c, at, :].astype(jnp.float32) + value).astype(out.dtype)
-
-    one = reduce_events(
-        order, places, lambda c, b: blocks.at[b, c], lambda c, b, at: blocks[b, c, at, :], put,
-        slots, sums, resid.shape[1], send, recv, events,
-    )
-    run_events(events, (one,))
-
-
-def collect(blocks, resid, sizes):
-    order = timed(ep_tree(sizes), 1.06, LAG_EP)
-    _, _, rows, cols = blocks.shape
-    bf16 = blocks.dtype
-    return pl.pallas_call(
-        functools.partial(collect_kernel, order, sizes),
-        out_shape=jax.ShapeDtypeStruct(resid.shape, bf16),
-        in_specs=vmem(2),
-        out_specs=vmem(1)[0],
-        scratch_shapes=[pltpu.VMEM((len(order), rows, cols), bf16)] * 2 + dma_sems(order),
-        compiler_params=params(5),
-        name="collect",
-    )(blocks, resid)
+        name="backward",
+    )(partial, extra_all, hid_all, down, resid)
 
 
 def split_up(x, dim, peers):
@@ -743,12 +817,8 @@
     reads, new_states = state_step(
         drive, states, decay_rate, frequency, log_step, b_real, b_imag, c_real, c_imag, skip_gain
     )
-    token_cols = lax.dynamic_slice_in_dim(tokens, tp_index * part_width, part_width, 1)
-    gain_cols = lax.dynamic_slice_in_dim(ffn_gain, tp_index * part_width, part_width, 0)[None]
-    gate_cols = lax.dynamic_slice_in_dim(branch_gate, tp_index * part_width, part_width, 0)
     normed_two, resid, branch = mix(
-        reads, out_cols, token_cols, gain_cols, gate_cols.astype(f32)[None], route_rows,
-        tp_count, width
+        reads, out_cols, tokens, ffn_gain[None], branch_gate[None], route_rows, tp_count, width
     )
     sizes = (lax.axis_size("ep_0"), lax.axis_size("ep_1"))
     both_proj = jnp.concatenate([dense_gate, dense_up], axis=1)
@@ -756,40 +826,11 @@
         normed_two, branch, both_proj, expert_gate[0], expert_up[0], expert_down[0],
         sizes, tp_count, capacity,
     )
-    dense_hidden = dense_hidden.reshape(ep_count * seq_count, -1)
-    spare = dense_hidden.shape[1] - dense_down.shape[0]
+    spare = dense_hidden.shape[3] - dense_down.shape[0]
     dense_down = jnp.pad(dense_down, ((0, spare), (0, 0)))
-    route_all = branch_all[:, 1:, :seq_count]
-    match = (route_all[:, :top_count] == ep_index.astype(f32)).astype(f32)
-    named = jnp.sum(match, axis=1)
-    weight_all = jnp.sum(match * route_all[:, top_count : 2 * top_count], axis=1).reshape(-1)
-    order = jnp.arange(seq_count)
-    before = (order[:, None] < order[None, :]).astype(f32)
-    slot = jnp.dot(named, before, preferred_element_type=f32)
-    group = jnp.arange(ep_count, dtype=jnp.int32) // sizes[1]
-    offset = lax.rem(lax.axis_index("ep_0") - group + sizes[0], sizes[0])
-    rank = jnp.zeros((ep_count,), f32)
-    for at, (dz, _, _) in enumerate(forward_plan(sizes, tp_count)[2]):
-        rank = jnp.where(offset == dz % sizes[0], float(at), rank)
-    within = (jnp.arange(ep_count, dtype=jnp.int32) % sizes[1]).astype(f32)
-    place = slot + capacity * (rank * sizes[1] + within)[:, None]
-    place = jnp.where(named > 0, place, -1.0).reshape(-1)
-    select = place[None, :] == jnp.arange(slots, dtype=f32)[:, None]
-    select = select.astype(bf16)
-    row_weight = jnp.sum(select.astype(f32) * weight_all[None, :], axis=1)
-    branch_all = branch_all[:, 0, :seq_count].reshape(ep_count * seq_count, 1)
-
-    row_weight = jnp.broadcast_to(row_weight[:, None], (slots, 128)).reshape(2, slots // 2, 128)
-    weighted = expert_out(partial, row_weight, tp_count)
-    weighted = weighted.reshape(slots, part_width)
-
-    dense_part = jnp.dot(dense_hidden, dense_down, preferred_element_type=f32)
-    routed = lax.dot_general(select, weighted, (((0,), (0,)), ((), ())), preferred_element_type=f32)
-    mine = (routed + branch_all * dense_part).astype(bf16)
-    output = collect(
-        mine.reshape(ep_count, 2, seq_count // 2, part_width),
-        resid.reshape(2, seq_count // 2, part_width),
-        sizes,
+    output = backward(
+        partial, branch_all, dense_hidden, dense_down,
+        resid.reshape(2, seq_count // 2, part_width), sizes, tp_count, capacity,
     )
     return (output.reshape(seq_count, part_width), new_states)
 

time: 177 us -> 158 us (0.89)
  Pallas kernels: 140 us -> 129 us
  matrix products: 8.74 us -> 4.33 us
  other arithmetic: 6.68 us -> 3.34 us
    pallas_call x2 -> x1, Pallas kernels: 55.2 us -> 44.1 us  [backward(): pl.pallas_call(functools.partial(backward_kernel, big, flows, start, spot...]
    dot_general x3 -> x0, matrix products: 5.75 us -> none  [the longest x1 2.97 us: shards(): lax.dot_general(select, weighted, (((0,), (0,)), ((), ())), preferred_ele...]
    dynamic_slice x2 -> x0, local copies, waits for them, and re-layouts: 2.87 us -> none  [the longest x1 1.54 us: shards(): lax.dynamic_slice_in_dim(tokens, tp_index * part_width, part_width, 1)]
    reduce_sum x2 -> x0, other arithmetic: 1.94 us -> none  [the longest x1 1.1 us: shards(): named = jnp.sum(match, axis=1)]
    unnamed x33 -> x31, local copies, waits for them, and re-layouts: 4.7 us -> 3.77 us
  transfers between devices with their start and end apart: 1 -> 1, of which waited for: 0 -> 0; matrix products, arithmetic and copies ran while one was open for 9% -> 10% of each run, Pallas kernels for 0% -> 0%
where the time goes in v3:
time: 158 us; the launch traced here: 157 us
  Pallas kernels  129 us (82%)
  local copies, waits for them, and re-layouts  13.6 us (9%)
  starting transfers between devices  5.75 us (4%)
  matrix products  4.33 us (3%)
  other arithmetic  3.34 us (2%)
    pallas_call x1, Pallas kernels, forward(): pl.pallas_call(functools.partial(forward_kernel, big, small, flows, sizes...  71.4 us
    pallas_call x1, Pallas kernels, backward(): pl.pallas_call(functools.partial(backward_kernel, big, flows, start, spot...  44.1 us
    pallas_call x1, Pallas kernels, mix(): pl.pallas_call(functools.partial(mix_kernel, tp_count, width), out_shape=...  13.3 us
    all_to_all x1, starting transfers between devices, shards(): lax.all_to_all(split_up(out_proj, 1, tp_count), 'tp', 0, 0, tiled=True)  5.75 us
    unnamed x31, local copies, waits for them, and re-layouts  3.77 us
  transfers between devices with their start and end apart: 1, of which 0 were waited for; matrix products, arithmetic and copies ran while one was open for 10% of the time, Pallas kernels for 0%

profile of v3, /device:TPU:8, one launch (start us, length us, event | category | flops | bytes accessed | tf_op | source)
XLA Modules:
  0.0 156.7 jit_solution(16134219504627127180)
XLA Ops:
  0.6 0.0 copy-start
  0.6 2.4 %copy.51 = bf16[16,8,8,512]{3,2,0,1:T(8,128)(2,1)} copy(bf16[16,8,8,512]{3,2,1,0:T(8,128)(2,1)} %bitcast.53) | data formatting | bytes 2097152 | tf_op jit(solution)/shard_map/reshape | solution.py:722
  3.0 5.8 %all-to-all-start = ((bf16[8,128,512]{2,1,0:T(8,128)(2,1)}), bf16[8,128,512]{2,1,0:T(8,128)(2,1)S(1)}, u32[]{:S(2)}, u32[]{:S(2)}) async-start(bf16[8,128,512]{2,1,0:T(8,128)(2,1)} %bitcast.42), calls=%async_computation | async-start | bytes 2097152 | tf_op jit(solution)/shard_map/all_to_all | solution.py:812
  8.8 0.0 copy-done.13
  8.8 0.5 exp.9
  9.3 1.7 %fusion.29 = (f32[1,96,512]{2,1,0:T(8,128)S(1)}, f32[1,96,512]{2,1,0:T(8,128)}) fusion(f32[2,96,512]{2,1,0:T(8,128)} %param.39), kind=kLoop, calls=%fused_computation.48 | loop fusion | bytes 786432 | tf_op jit(solution)/shard_map/slice | solution.py:752
  11.0 0.1 copy.36
  11.1 1.1 copy.37
  12.2 0.0 copy-done.2
  12.2 0.0 copy-start.9
  12.2 0.0 copy-start.10
  12.2 0.0 copy-start.3
  12.3 0.0 copy-start.4
  12.3 0.3 fusion
  12.5 0.0 copy-done
  12.5 1.8 %convolution_convert_fusion = bf16[96,128]{1,0:T(8,128)(2,1)} fusion(bf16[4096,128]{1,0:T(8,128)(2,1)S(1)} %copy-done, bf16[96,4096]{1,0:T(8,128)(2,1)S(1)} %copy-done.2, f32[4096]{0:T(1024)} %param.28, f32[96]{0:T(128)S(1)} %add_rsqrt_fusion), kind=kOutput, calls=%fused_computation.12 | convolution fusion | flops 102248448 | bytes 1876352 | tf_op jit(solution)/shard_map/dot_general | solution.py:816
  14.3 0.9 copy.38
  15.2 0.0 copy-done.9
  15.2 0.0 copy-done.10
  15.2 0.7 add_divide_fusion
  15.9 0.0 copy-done.3
  16.0 0.3 fusion.3
  16.3 0.3 fusion.4
  16.6 0.0 copy-done.12
  16.6 0.0 copy-start.7
  16.6 0.1 mul.176
  16.7 1.0 fusion.30
  17.6 1.0 fusion.6
  18.6 0.0 copy-done.11
  18.7 0.1 copy.43
  18.8 0.6 broadcast_in_dim.5.gate
  19.4 0.1 copy.45
  19.5 1.1 copy.46
  20.6 0.1 copy.48
  20.7 0.1 copy.47
  20.8 0.0 copy-done.7
  20.9 1.6 %pad.13.down = bf16[256,512]{1,0:T(8,128)(2,1)} pad(bf16[192,512]{1,0:T(8,128)(2,1)} %param.48, bf16[]{:T(256)} %constant.80.clone.1), padding=0_64x0_0 | pad | bytes 458754 | tf_op jit(solution)/shard_map/jit(_pad)/pad | solution.py:830
  22.5 0.5 scatter.9.route
  23.1 0.9 pad_maximum_fusion.both
  24.0 0.8 pad_maximum_fusion.1
  24.7 0.6 fusion.23.reads
  25.4 0.0 all-to-all-done
  25.4 0.0 copy-done.6
  25.4 1.0 copy-done.1
  26.3 13.3 %mix.1 = (bf16[2,48,512]{2,1,0:T(8,128)(2,1)}, bf16[96,512]{1,0:T(8,128)(2,1)}, f32[8,128]{1,0:T(8,128)}) custom-call(bf16[96,128]{1,0:T(8,128)(2,1)} %fusion.23.reads, bf16[1024,512]{1,0:T(8,128)(2,1)} %bitcast.43, bf16[96,4096]{1,0:T(8,128)(2,1)} %tokens.1, f32[1,4096]{1,0:T(1,128)} %bitcast.60, bf16[1,4096]{1,0:T(2,128)(2,1)} %broadcast_in_dim.5.gate, ...), custom_call_target="tpu_custom_call" | custom-call | tf_op jit(solution)/shard_map/mix/pallas_call | solution.py:334
  39.6 71.4 %forward.1 = (bf16[2,192,4096]{2,1,0:T(8,128)(2,1)}, bf16[8,8,48,256]{3,2,1,0:T(8,128)(2,1)}, f32[32,8,128]{2,1,0:T(8,128)}) custom-call(bf16[2,48,512]{2,1,0:T(8,128)(2,1)} %get-tuple-element.32.block, f32[8,128]{1,0:T(8,128)} %get-tuple-element.33.extra, bf16[512,384]{1,0:T(8,128)(2,1)} %pad_maximum_fusion.both, bf16[4096,384]{1,0:T(8,128)(2,1)} %bitcast.44, ...), custom_call_target="tpu_custom_call" | custom-call | tf_op jit(solution)/shard_map/forward/pallas_call | solution.py:553
  111.0 44.1 %backward.1 = bf16[2,48,512]{2,1,0:T(8,128)(2,1)} custom-call(bf16[2,192,4096]{2,1,0:T(8,128)(2,1)} %get-tuple-element.34.partial, f32[32,8,128]{2,1,0:T(8,128)} %get-tuple-element.35.extra_all, bf16[8,8,48,256]{3,2,1,0:T(8,128)(2,1)} %get-tuple-element.36.hid_all, bf16[256,512]{1,0:T(8,128)(2,1)} %pad.13.down, bf16[2,48,512]{2,1,0:T(8,128)(2,1)} %bitcast.59), custom_call_target="tpu_custom_call" | custom-call | tf_op jit(solution)/shard_map/backward/pallas_call | solution.py:697
  155.1 1.5 copy.54
  (17 shorter events, 0.1 us)
Async XLA Ops:
  0.6 11.9 %copy-start = (bf16[4096,128]{1,0:T(8,128)(2,1)S(1)}, bf16[4096,128]{1,0:T(8,128)(2,1)}, u32[]{:S(2)}) copy-start(bf16[4096,128]{1,0:T(8,128)(2,1)} %param.30) | copy-start | bytes 3145732
  3.0 5.8 %copy-start.13 = (f32[8]{0:T(128)S(1)}, f32[8]{0:T(128)}, u32[]{:S(2)}) copy-start(f32[8]{0:T(128)} %param.33) | copy-start | bytes 100
  3.0 9.2 %copy-start.2 = (bf16[96,4096]{1,0:T(8,128)(2,1)S(1)}, bf16[96,4096]{1,0:T(8,128)(2,1)}, u32[]{:S(2)}) copy-start(bf16[96,4096]{1,0:T(8,128)(2,1)} %tokens.1) | copy-start | bytes 2359300
  3.0 22.3 %all-to-all-start = ((bf16[8,128,512]{2,1,0:T(8,128)(2,1)}), bf16[8,128,512]{2,1,0:T(8,128)(2,1)S(1)}, u32[]{:S(2)}, u32[]{:S(2)}) async-start(bf16[8,128,512]{2,1,0:T(8,128)(2,1)} %bitcast.42), calls=%async_computation | async-start | bytes 2097152 | tf_op jit(solution)/shard_map/all_to_all | solution.py:812
  12.2 3.0 %copy-start.9 = (f32[8,64]{1,0:T(8,128)S(1)}, f32[8,64]{1,0:T(8,128)}, u32[]{:S(2)}) copy-start(f32[8,64]{1,0:T(8,128)} %param.32) | copy-start | bytes 6148
  12.2 3.0 %copy-start.10 = (f32[8,64]{1,0:T(8,128)S(1)}, f32[8,64]{1,0:T(8,128)}, u32[]{:S(2)}) copy-start(f32[8,64]{1,0:T(8,128)} %param.31) | copy-start | bytes 6148
  12.2 3.7 %copy-start.3 = (f32[8,64,16]{1,2,0:T(8,128)S(1)}, f32[8,64,16]{1,2,0:T(8,128)}, u32[]{:S(2)}) copy-start(f32[8,64,16]{1,2,0:T(8,128)} %param.35) | copy-start | bytes 98308
  12.3 3.7 %copy-start.4 = (f32[8,64,16]{1,2,0:T(8,128)S(1)}, f32[8,64,16]{1,2,0:T(8,128)}, u32[]{:S(2)}) copy-start(f32[8,64,16]{1,2,0:T(8,128)} %param.34) | copy-start | bytes 98308
  14.3 2.3 %copy-start.12 = (f32[128]{0:T(128)S(1)}, f32[128]{0:T(128)}, u32[]{:S(2)}) copy-start(f32[128]{0:T(128)} %param.38) | copy-start | bytes 1540
  14.3 4.3 %copy-start.11 = (s32[96,2]{0,1:T(2,128)S(1)}, s32[96,2]{0,1:T(2,128)}, u32[]{:S(2)}) copy-start(s32[96,2]{0,1:T(2,128)} %param.41) | copy-start | bytes 2308
  14.3 4.4 %copy-start.8 = (bf16[4096]{0:T(1024)(128)(2,1)S(1)}, bf16[4096]{0:T(1024)(128)(2,1)}, u32[]{:S(2)}) copy-start(bf16[4096]{0:T(1024)(128)(2,1)} %param.49) | copy-start | bytes 24580
  14.3 5.1 %copy-start.5 = (bf16[512,192]{0,1:T(8,128)(2,1)S(1)}, bf16[512,192]{0,1:T(8,128)(2,1)}, u32[]{:S(2)}) copy-start(bf16[512,192]{0,1:T(8,128)(2,1)} %param.46) | copy-start | bytes 589828
  16.6 4.3 %copy-start.7 = (f32[96,2]{0,1:T(2,128)S(1)}, f32[96,2]{0,1:T(2,128)}, u32[]{:S(2)}) copy-start(f32[96,2]{0,1:T(2,128)} %param.42) | copy-start | bytes 2308
  23.0 2.3 %copy-start.6 = (f32[8,128]{1,0:T(8,128)}, f32[8,128]{1,0:T(8,128)S(1)}, u32[]{:S(2)}) copy-start(f32[8,128]{1,0:T(8,128)S(1)} %scatter.9.route) | copy-start | bytes 12292
  25.4 1.0 copy-start.1
